TPU v7x, 32 devices: a whole 2x2x4 slice. The times are simulated.
32 devices in a mesh: sp: 8 (over z, x), tp: 4 (over y, core).
Axes of the slice: x: 2, y: 2, z: 4, core: 2. Of those that a mesh axis runs over, the one named last changes fastest.
Arguments:
- residual: bfloat16 [1024, 2048], P('sp'), may hold values from -6 to 6
- query_narrow: bfloat16 [1024, 1024], P('sp', 'tp'), may hold values from -6 to 6
- keys_narrow: bfloat16 [1024, 1024], P('sp', 'tp'), may hold values from -6 to 6
- values_narrow: bfloat16 [1024, 1024], P('sp', 'tp'), may hold values from -6 to 6
- outgate_narrow: bfloat16 [1024, 1024], P('sp', 'tp'), may hold values from -6 to 6
- gates_narrow: float32 [4, 8, 1024], P(None, 'tp', 'sp'), may hold values from -4 to 100
- query_broad: bfloat16 [1024, 1024], P('sp', 'tp'), may hold values from -6 to 6
- keys_broad: bfloat16 [1024, 1024], P('sp', 'tp'), may hold values from -6 to 6
- values_broad: bfloat16 [1024, 1024], P('sp', 'tp'), may hold values from -6 to 6
- outgate_broad: bfloat16 [1024, 1024], P('sp', 'tp'), may hold values from -6 to 6
- gates_broad: float32 [4, 4, 1024], P(None, 'tp', 'sp'), may hold values from -4 to 100
- outproj_narrow: bfloat16 [1024, 2048], P('tp'), may hold values from -0.125 to 0.125
- outproj_broad: bfloat16 [1024, 2048], P('tp'), may hold values from -0.125 to 0.125
- norm_gain: bfloat16 [2048], replicated, may hold values from 0.099609375 to 1.8984375
- gate_weight: bfloat16 [2048, 5632], P('sp', 'tp'), may hold values from -0.125 to 0.125
- up_weight: bfloat16 [2048, 5632], P('sp', 'tp'), may hold values from -0.125 to 0.125
- down_weight: bfloat16 [2048, 5632], P('sp', 'tp'), may hold values from -0.078125 to 0.078125
Outputs:
- layer_out: bfloat16 [1024, 2048], P(('sp', 'tp'))
All inputs are finite; a program needn't handle non-finite values.
Results may differ from a plain program's by a relative error of at most 0.0085.
Values may be sent and summed in bfloat16 or wider, within the bound.
A program may use at most 192 MiB of HBM per device.

v0:
```python
import functools

import jax
import jax.numpy as jnp
from jax import lax
from jax.experimental import pallas as pl
from jax.experimental.pallas import tpu as pltpu
from jax.sharding import PartitionSpec as P

DH_A = 128
DH_B = 256

EPSILON = 1e-06
FAR = -1e30
MESH = pl.DeviceIdType.MESH


def direction_columns(in_gate, log_forget, reverse):
    place, length = lax.axis_index("sp"), lax.axis_size("sp")
    cumulative = lax.cumsum(log_forget, axis=1, reverse=reverse)
    total = cumulative[:, 0] if reverse else cumulative[:, -1]
    toward_end = total[:, None] - cumulative + in_gate
    packed = jnp.concatenate([toward_end, total[:, None]], axis=1)
    every = lax.all_gather(packed, "sp")
    ends, totals = every[:, :, :-1], every[:, :, -1]
    index = jnp.arange(length)
    if reverse:
        between = (index[None, :] > place) & (index[None, :] < index[:, None])
        valid = index > place
    else:
        between = (index[None, :] < place) & (index[None, :] > index[:, None])
        valid = index < place
    offset = jnp.sum(jnp.where(between[:, :, None], totals[None], 0.0), axis=1)
    columns = jnp.where(valid[:, None, None], offset[:, :, None] + ends, FAR)
    own = (in_gate - cumulative)[None]
    columns = jnp.where((index == place)[:, None, None], own, columns)
    return jnp.moveaxis(columns, 0, 1).reshape(in_gate.shape[0], -1)


def group_cell(query, keys, values, outgate, gates, width):
    rows, every = query.shape[0], keys.shape[0]
    place = lax.axis_index("sp")
    heads = query.shape[1] // width
    q = query.reshape(rows, heads, width)
    k = keys.reshape(every, heads, width)
    v = values.reshape(every, heads, width)
    scores = jnp.einsum("thd,shd->hts", q, k, preferred_element_type=jnp.float32) * width ** (-0.5)
    t_at = (place * rows + jnp.arange(rows))[:, None]
    s_at = jnp.arange(every)[None, :]
    summed = 0.0
    for direction in range(2):
        columns = direction_columns(
            gates[direction], jax.nn.log_sigmoid(gates[2 + direction]), direction == 1
        )
        mask = s_at >= t_at if direction else s_at <= t_at
        log_weight = jnp.where(mask[None], columns[:, None, :], FAR)
        top = jnp.max(log_weight, axis=2, keepdims=True)
        weighted = jnp.exp(log_weight - top) * scores
        den = jnp.sum(weighted, axis=2)
        num = jnp.einsum(
            "hts,shd->thd", weighted.astype(jnp.bfloat16), v, preferred_element_type=jnp.float32
        )
        summed = summed + num / jnp.maximum(jnp.abs(jnp.transpose(den)), 1.0)[:, :, None]
    normed = summed * lax.rsqrt(jnp.mean(summed * summed, axis=2, keepdims=True) + EPSILON)
    return (normed.reshape(rows, -1) * jax.nn.sigmoid(outgate.astype(jnp.float32))).astype(
        jnp.bfloat16
    )


def shards(
    residual,
    query_narrow,
    keys_narrow,
    values_narrow,
    outgate_narrow,
    gates_narrow,
    query_broad,
    keys_broad,
    values_broad,
    outgate_broad,
    gates_broad,
    outproj_narrow,
    outproj_broad,
    norm_gain,
    gate_weight,
    up_weight,
    down_weight,
):
    spread = lax.axis_size("sp")
    channels, hidden_own = gate_weight.shape
    stacked = jnp.stack([gate_weight.T, up_weight.T, down_weight.T])
    pieces = stacked.reshape(3, spread, hidden_own // spread, channels)
    pieces = lax.all_to_all(pieces, "sp", split_axis=1, concat_axis=1)
    weights = jnp.swapaxes(pieces, 1, 2).reshape(3, hidden_own // spread, -1)

    narrow, broad = keys_narrow.shape[1], keys_broad.shape[1]
    memory = lax.all_gather(
        jnp.concatenate([keys_narrow, values_narrow, keys_broad, values_broad], axis=1),
        "sp",
        axis=0,
        tiled=True,
    )
    kn, vn = memory[:, :narrow], memory[:, narrow : 2 * narrow]
    kb, vb = memory[:, 2 * narrow : 2 * narrow + broad], memory[:, 2 * narrow + broad :]
    cell_narrow = group_cell(query_narrow, kn, vn, outgate_narrow, gates_narrow, DH_A)
    cell_broad = group_cell(query_broad, kb, vb, outgate_broad, gates_broad, DH_B)

    own_count = residual.shape[0] // lax.axis_size("tp")
    proj = lax.psum_scatter(
        (
            jnp.dot(cell_narrow, outproj_narrow, preferred_element_type=jnp.float32)
            + jnp.dot(cell_broad, outproj_broad, preferred_element_type=jnp.float32)
        ).astype(jnp.bfloat16),
        "tp",
        scatter_dimension=0,
        tiled=True,
    ).astype(jnp.float32)
    offset = lax.axis_index("tp") * own_count
    stream = lax.dynamic_slice_in_dim(residual, offset, own_count, 0).astype(jnp.float32) + proj
    scaled = stream * lax.rsqrt(jnp.mean(stream * stream, axis=1, keepdims=True) + EPSILON)
    normed = (scaled * norm_gain.astype(jnp.float32)).astype(jnp.bfloat16)
    normed = lax.all_gather(normed, ("sp", "tp"), axis=0, tiled=True)
    nt = (((1,), (1,)), ((), ()))
    gate = lax.dot_general(normed, weights[0], nt, preferred_element_type=jnp.float32)
    upward = lax.dot_general(normed, weights[1], nt, preferred_element_type=jnp.float32)
    hidden = (jax.nn.silu(gate) * upward).astype(jnp.bfloat16)
    partial_value = jnp.dot(hidden, weights[2], preferred_element_type=jnp.float32)
    ffn = lax.psum_scatter(
        partial_value.astype(jnp.bfloat16), ("sp", "tp"), scatter_dimension=0, tiled=True
    ).astype(jnp.float32)
    return (stream + 0.5 * ffn).astype(jnp.bfloat16)


def fused_kernel(geometry, *refs):
    spread, members, wide, narrow_heads, broad_heads = geometry
    (res, qn, kn, vn, on, gn, qb, kb, vb, ob, gb, opn, opb, gain, gw, uw, dw, out) = refs[:18]
    (kv_all, info, gates, wt, w_all, pp, rs, x_all, part, r1l, r1r, s1l, s1r, r2l, r2r, s2, r3) = (
        refs[18:35]
    )
    (kv_send, kv_recv, in_send, in_recv, w_send, w_recv, f_send, f_recv) = refs[35:43]
    (p_send, p_recv, x_send, x_recv, e_send, e_recv, z_send, z_recv) = refs[43:51]
    rows = res.shape[0]
    own = rows // members
    depth, tall = spread // 2, members // 2
    chan, hid = gw.shape
    piece = hid // spread
    ca, cb = kn.shape[1], kb.shape[1]
    half = res.shape[1] // 2
    i, j = lax.axis_index("sp"), lax.axis_index("tp")
    z, x = i // 2, i % 2
    y, c = j // 2, j % 2
    ox, oy = 1 - x, 1 - y
    f32, bf16 = jnp.float32, jnp.bfloat16
    pending = []

    def send(src, dst, s_sem, r_sem, to, cond=None):
        copy = pltpu.make_async_remote_copy(
            src_ref=src, dst_ref=dst, send_sem=s_sem, recv_sem=r_sem, device_id=to, device_id_type=MESH
        )
        copy.start()
        return copy

    def arrived(ref, sem):
        pltpu.make_async_remote_copy(
            src_ref=ref, dst_ref=ref, send_sem=sem, recv_sem=sem, device_id=(i, j), device_id_type=MESH
        ).wait_recv()

    def sent(ref, sem, cond=None):
        def wait():
            pltpu.make_async_remote_copy(
                src_ref=ref, dst_ref=ref, send_sem=sem, recv_sem=sem, device_id=(i, j), device_id_type=MESH
            ).wait_send()

        if cond is None:
            wait()
        else:
            pl.when(cond)(wait)

    barrier = pltpu.get_barrier_semaphore()
    for k in range(1, spread):
        pl.semaphore_signal(barrier, inc=1, device_id=((i + k) % spread, j), device_id_type=MESH)
    for k in range(1, members):
        pl.semaphore_signal(barrier, inc=1, device_id=(i, (j + k) % members), device_id_type=MESH)

    kv_all[i, :, 0:ca] = kn[...]
    kv_all[i, :, ca : 2 * ca] = vn[...]
    kv_all[i, :, 2 * ca : 2 * ca + cb] = kb[...]
    kv_all[i, :, 2 * ca + cb : 2 * ca + 2 * cb] = vb[...]
    gates[...] = jnp.zeros_like(gates)
    for role in range(4):
        at = 8 * (role % 2)
        gates[role // 2, at : at + narrow_heads, :] = gn[role]
        gates[role // 2, at + narrow_heads : at + narrow_heads + broad_heads, :] = gb[role]
    in_gate, pre = gates[0], gates[1]
    forget = jnp.minimum(pre, 0.0) - jnp.log1p(jnp.exp(-jnp.abs(pre)))
    r_at = lax.broadcasted_iota(jnp.int32, (rows, rows), 0)
    c_at = lax.broadcasted_iota(jnp.int32, (rows, rows), 1)
    run = lambda m: jnp.dot(
        forget, m.astype(f32), preferred_element_type=f32, precision=lax.Precision.HIGHEST
    )
    forward_row = lax.broadcasted_iota(jnp.int32, in_gate.shape, 0) < 8
    cumulative = jnp.where(forward_row, run(r_at <= c_at), run(r_at >= c_at))
    total = jnp.where(
        forward_row,
        jnp.broadcast_to(cumulative[:, rows - 1 : rows], in_gate.shape),
        jnp.broadcast_to(cumulative[:, 0:1], in_gate.shape),
    )
    own_column = in_gate - cumulative
    info[i, 0] = total + own_column
    info[i, 1] = total
    pl.semaphore_wait(barrier, spread + members - 2)

    def pass_kv(slot, way, to):
        send(kv_all.at[slot], kv_all.at[slot], kv_send.at[way, slot], kv_recv.at[slot], to)
        send(info.at[slot], info.at[slot], in_send.at[way, slot], in_recv.at[slot], to)

    def kv_arrived(slot):
        arrived(kv_all.at[slot], kv_recv.at[slot])
        arrived(info.at[slot], in_recv.at[slot])

    @pl.when(z + 1 < depth)
    def _():
        pass_kv(i, 0, (i + 2, j))

    @pl.when(z >= 1)
    def _():
        pass_kv(i, 1, (i - 2, j))

    pass_kv(i, 2, (2 * z + ox, j))

    for m, ref in enumerate((gw, uw, dw)):
        for k in range(hid // 128):
            wt[m, k * 128 : (k + 1) * 128, :] = ref[:, k * 128 : (k + 1) * 128].T
    mine = pl.ds(pl.multiple_of(i * piece, 16), piece)
    columns = pl.ds(pl.multiple_of(i * chan, 128), chan)
    w_all[:, c, :, columns] = wt[:, mine, :]

    for s in range(1, depth):

        @pl.when(z - s >= 0)
        def _():
            slot = i - 2 * s
            kv_arrived(slot)

            @pl.when(z + 1 < depth)
            def _():
                pass_kv(slot, 0, (i + 2, j))

            pass_kv(slot, 2, (2 * z + ox, j))

        @pl.when(z + s < depth)
        def _():
            slot = i + 2 * s
            kv_arrived(slot)

            @pl.when(z >= 1)
            def _():
                pass_kv(slot, 1, (i - 2, j))

            pass_kv(slot, 2, (2 * z + ox, j))

    sibling = (i, j + 1 - 2 * c)
    send(wt.at[:, mine, :], w_all.at[:, c, :, columns], f_send.at[i], f_recv.at[i], sibling)
    order = list(range(1, spread, 2)) + list(range(2, spread, 2))
    early = len(order) - len(order) // 3

    def send_weights(k):
        p = (i + k) % spread
        theirs = pl.ds(pl.multiple_of(p * piece, 16), piece)
        send(wt.at[:, theirs, :], w_all.at[:, c, :, columns], w_send.at[p], w_recv.at[i], (p, j))

    for k in order[:early]:
        send_weights(k)

    for zz in range(depth):
        kv_arrived(2 * zz + ox)

    offset = jnp.zeros_like(total)
    pieces = [None] * spread
    forward_sum = jnp.zeros_like(total)
    ahead = [None] * spread
    for k in reversed(range(spread)):
        ahead[k] = forward_sum
        forward_sum = forward_sum + jnp.where(k < i, info[k, 1], 0.0)
    backward_sum = jnp.zeros_like(total)
    for k in range(spread):
        reach = jnp.where(forward_row, ahead[k], backward_sum) + info[k, 0]
        seen = jnp.logical_or(
            jnp.logical_and(forward_row, k < i), jnp.logical_and(jnp.logical_not(forward_row), k > i)
        )
        pieces[k] = jnp.where(k == i, own_column, jnp.where(seen, reach, FAR))
        backward_sum = backward_sum + jnp.where(k > i, info[k, 1], 0.0)
    column = jnp.concatenate(pieces, axis=1)
    t_at = lax.broadcasted_iota(jnp.int32, (rows, spread * rows), 0) + i * rows
    s_at = lax.broadcasted_iota(jnp.int32, (rows, spread * rows), 1)
    masks = (s_at <= t_at, s_at >= t_at)
    nt = (((1,), (1,)), ((), ()))
    proj = jnp.zeros((rows, res.shape[1]), f32)
    heads = [(qn, on, opn, 0, ca, h, ca // narrow_heads, h) for h in range(narrow_heads)]
    heads += [
        (qb, ob, opb, 2 * ca, cb, h, cb // broad_heads, narrow_heads + h) for h in range(broad_heads)
    ]
    for query, outgate, outproj, base, group, h, width, row in heads:
        lanes = slice(h * width, (h + 1) * width)
        keys = kv_all[:, :, base + h * width : base + (h + 1) * width].reshape(spread * rows, width)
        vals = kv_all[:, :, base + group + h * width : base + group + (h + 1) * width].reshape(
            spread * rows, width
        )
        scores = lax.dot_general(query[:, lanes], keys, nt, preferred_element_type=f32) * width ** (-0.5)
        summed = jnp.zeros((rows, width), f32)
        for direction in range(2):
            at = 8 * direction + row
            weight = jnp.where(
                masks[direction],
                jnp.broadcast_to(column[at : at + 1, :], scores.shape),
                FAR,
            )
            top = jnp.max(weight, axis=1, keepdims=True)
            p = jnp.exp(weight - top) * scores
            den = jnp.sum(p, axis=1, keepdims=True)
            num = jnp.dot(p.astype(bf16), vals, preferred_element_type=f32)
            summed = summed + num / jnp.maximum(jnp.abs(den), 1.0)
        normed = summed * lax.rsqrt(jnp.mean(summed * summed, axis=1, keepdims=True) + EPSILON)
        opened = 1.0 / (1.0 + jnp.exp(-outgate[:, lanes].astype(f32)))
        cell = (normed * opened).astype(bf16)
        proj = proj + jnp.dot(cell, outproj[lanes, :], preferred_element_type=f32)
    pp[...] = proj.astype(bf16).reshape(pp.shape)

    for k in range(1, members):
        q = (j + k) % members
        send(pp.at[q], rs.at[j], p_send.at[q], p_recv.at[j], (i, q))
    stream = res[pl.ds(pl.multiple_of(j * own, own), own), :].astype(f32) + pp[j].astype(f32)
    for k in range(1, members):
        q = (j + k) % members
        arrived(rs.at[q], p_recv.at[q])
        stream = stream + rs[q].astype(f32)
    scaled = stream * lax.rsqrt(jnp.mean(stream * stream, axis=1, keepdims=True) + EPSILON)
    x_all[x, y, z] = (scaled * gain[...].astype(f32)).astype(bf16)

    def pass_x(xx, yy, zz, way, to):
        slot = x_all.at[xx, yy, zz]
        send(slot, slot, x_send.at[way, xx, yy, zz], x_recv.at[xx, yy, zz], to)

    def x_arrived(xx, yy, zz):
        arrived(x_all.at[xx, yy, zz], x_recv.at[xx, yy, zz])

    x_peer, y_peer = (2 * z + ox, j), (i, 2 * oy + c)

    @pl.when(z + 1 < depth)
    def _():
        pass_x(x, y, z, 0, (i + 2, j))

    @pl.when(z >= 1)
    def _():
        pass_x(x, y, z, 1, (i - 2, j))

    pass_x(x, y, z, 2, x_peer)
    pass_x(x, y, z, 3, y_peer)
    for s in range(1, depth):

        @pl.when(z - s >= 0)
        def _():
            x_arrived(x, y, z - s)

            @pl.when(z + 1 < depth)
            def _():
                pass_x(x, y, z - s, 0, (i + 2, j))

            pass_x(x, y, z - s, 2, x_peer)
            pass_x(x, y, z - s, 3, y_peer)

        @pl.when(z + s < depth)
        def _():
            x_arrived(x, y, z + s)

            @pl.when(z >= 1)
            def _():
                pass_x(x, y, z + s, 1, (i - 2, j))

            pass_x(x, y, z + s, 2, x_peer)
            pass_x(x, y, z + s, 3, y_peer)

    for k in order[early:]:
        send_weights(k)

    for zz in range(depth):
        x_arrived(x, oy, zz)
        if zz < depth // 2:
            pass_x(x, oy, zz, 2, x_peer)
        x_arrived(ox, y, zz)
        if zz >= depth // 2:
            pass_x(ox, y, zz, 3, y_peer)

    for k in order:
        p = (i + spread - k) % spread
        theirs = pl.ds(pl.multiple_of(p * chan, 128), chan)
        slot = w_all.at[:, c, :, theirs]
        arrived(slot, w_recv.at[p])
        send(slot, slot, f_send.at[p], f_recv.at[p], sibling)
    for k in [0] + order:
        p = (i + spread - k) % spread
        theirs = pl.ds(pl.multiple_of(p * chan, 128), chan)
        arrived(w_all.at[:, 1 - c, :, theirs], f_recv.at[p])

    units = 2 * piece

    def chunk(xx, yy):
        a = x_all[xx, yy].reshape(depth * own, -1)
        gate = lax.dot_general(a, w_all[0].reshape(units, -1), nt, preferred_element_type=f32)
        up = lax.dot_general(a, w_all[1].reshape(units, -1), nt, preferred_element_type=f32)
        hidden = (gate / (1.0 + jnp.exp(-gate)) * up).astype(bf16)
        got = jnp.dot(hidden, w_all[2].reshape(units, -1), preferred_element_type=f32)
        part[xx, yy] = got.astype(bf16).reshape(depth, own, -1)

    left, right = slice(0, half), slice(half, 2 * half)
    chunk(ox, y)
    for zz in range(depth):
        x_arrived(ox, oy, zz)
    chunk(ox, oy)
    send(part.at[ox, :, :, :, pl.ds(0, half)], r1l, e_send.at[0], e_recv.at[0], x_peer)
    chunk(x, oy)
    send(part.at[:, oy, :, :, pl.ds(half, half)], r1r, e_send.at[1], e_recv.at[1], y_peer)
    chunk(x, y)
    arrived(r1l, e_recv.at[0])
    s1l[...] = (part[x, :, :, :, left].astype(f32) + r1l[...].astype(f32)).astype(bf16)
    send(s1l.at[oy], r2l, e_send.at[2], e_recv.at[2], y_peer)
    arrived(r1r, e_recv.at[1])
    s1r[...] = (part[:, y, :, :, right].astype(f32) + r1r[...].astype(f32)).astype(bf16)
    send(s1r.at[ox], r2r, e_send.at[3], e_recv.at[3], x_peer)
    arrived(r2l, e_recv.at[2])
    s2[:, :, left] = (s1l[y].astype(f32) + r2l[...].astype(f32)).astype(bf16)
    arrived(r2r, e_recv.at[3])
    s2[:, :, right] = (s1r[x].astype(f32) + r2r[...].astype(f32)).astype(bf16)
    for k in range(1, depth):
        zz = (z + k) % depth
        send(s2.at[zz], r3.at[z], z_send.at[zz], z_recv.at[z], (2 * zz + x, j))
    ffn = s2[z].astype(f32)
    for k in range(1, depth):
        zz = (z + k) % depth
        arrived(r3.at[zz], z_recv.at[zz])
        ffn = ffn + r3[zz].astype(f32)
    out[...] = (stream + 0.5 * ffn).astype(out.dtype)

    def kv_sent(slot, way, cond=None):
        sent(kv_all.at[slot], kv_send.at[way, slot], cond)
        sent(info.at[slot], in_send.at[way, slot], cond)

    for zz in range(depth):
        kv_sent(2 * zz + x, 0, jnp.logical_and(zz <= z, z + 1 < depth))
        kv_sent(2 * zz + x, 1, jnp.logical_and(zz >= z, z >= 1))
        kv_sent(2 * zz + x, 2)
        slot = x_all.at[x, y, zz]
        sent(slot, x_send.at[0, x, y, zz], jnp.logical_and(zz <= z, z + 1 < depth))
        sent(slot, x_send.at[1, x, y, zz], jnp.logical_and(zz >= z, z >= 1))
        sent(slot, x_send.at[2, x, y, zz])
        sent(slot, x_send.at[3, x, y, zz])
        if zz < depth // 2:
            sent(slot, x_send.at[2, x, oy, zz])
        else:
            sent(slot, x_send.at[3, ox, y, zz])
    block = wt.at[:, mine, :]
    sent(block, f_send.at[i])
    for k in range(1, spread):
        p = (i + k) % spread
        sent(block, w_send.at[p])
        sent(block, f_send.at[p])
    for k in range(1, members):
        sent(rs.at[0], p_send.at[(j + k) % members])
    sent(r1l, e_send.at[0])
    sent(r1r, e_send.at[1])
    sent(r2l, e_send.at[2])
    sent(r2r, e_send.at[3])
    for k in range(1, depth):
        sent(r3.at[0], z_send.at[(z + k) % depth])


def fused_shards(*args):
    (res, qn, kn, vn, on, gn, qb, kb, vb, ob, gb, opn, opb, gain, gw, uw, dw) = args
    spread, members = lax.axis_size("sp"), lax.axis_size("tp")
    rows, wide = res.shape
    own, depth, tall = rows // members, spread // 2, members // 2
    chan, hid = gw.shape
    piece = hid // spread
    kvw = 2 * (kn.shape[1] + kb.shape[1])
    bf16, f32 = jnp.bfloat16, jnp.float32
    v = pltpu.VMEM
    dma = pltpu.SemaphoreType.DMA
    scratch = [
        v((spread, rows, kvw), bf16),
        v((spread, 2, 16, rows), f32),
        v((2, 16, rows), f32),
        v((3, hid, chan), bf16),
        v((3, 2, piece, wide), bf16),
        v((members, own, wide), bf16),
        v((members, own, wide), bf16),
        v((2, tall, depth, own, wide), bf16),
        v((2, tall, depth, own, wide), bf16),
        v((tall, depth, own, wide // 2), bf16),
        v((2, depth, own, wide // 2), bf16),
        v((tall, depth, own, wide // 2), bf16),
        v((2, depth, own, wide // 2), bf16),
        v((depth, own, wide // 2), bf16),
        v((depth, own, wide // 2), bf16),
        v((depth, own, wide), bf16),
        v((depth, own, wide), bf16),
        dma((3, spread)),
        dma((spread,)),
        dma((3, spread)),
        dma((spread,)),
        dma((spread,)),
        dma((spread,)),
        dma((spread,)),
        dma((spread,)),
        dma((members,)),
        dma((members,)),
        dma((4, 2, tall, depth)),
        dma((2, tall, depth)),
        dma((4,)),
        dma((4,)),
        dma((depth,)),
        dma((depth,)),
    ]
    geometry = (spread, members, wide, gn.shape[1], gb.shape[1])
    return pl.pallas_call(
        functools.partial(fused_kernel, geometry),
        out_shape=jax.ShapeDtypeStruct((own, wide), bf16),
        in_specs=[pl.BlockSpec(memory_space=pltpu.VMEM)] * 17,
        out_specs=pl.BlockSpec(memory_space=pltpu.VMEM),
        scratch_shapes=scratch,
        compiler_params=pltpu.CompilerParams(
            collective_id=0, has_side_effects=True, vmem_limit_bytes=60 * 1024 * 1024
        ),
        name="fused",
    )(res, qn, kn, vn, on, gn, qb, kb, vb, ob, gb, opn, opb, gain.reshape(1, -1), gw, uw, dw)


def pick(*args):
    res, kn, gn, gb, gw = args[0], args[2], args[5], args[10], args[14]
    spread, members = lax.axis_size("sp"), lax.axis_size("tp")
    rows = res.shape[0]
    chan, hid = gw.shape
    fits = (
        spread % 2 == 0
        and spread >= 4
        and members == 4
        and rows == 128
        and spread * rows <= 2048
        and chan % 128 == 0
        and hid % (16 * spread) == 0
        and hid % 128 == 0
        and gn.shape[1] + gb.shape[1] <= 8
    )
    return fused_shards(*args) if fits else shards(*args)


def solution(mesh):
    in_specs = (
        P("sp", None),
        P("sp", "tp"),
        P("sp", "tp"),
        P("sp", "tp"),
        P("sp", "tp"),
        P(None, "tp", "sp"),
        P("sp", "tp"),
        P("sp", "tp"),
        P("sp", "tp"),
        P("sp", "tp"),
        P(None, "tp", "sp"),
        P("tp", None),
        P("tp", None),
        P(),
        P("sp", "tp"),
        P("sp", "tp"),
        P("sp", "tp"),
    )
    out_specs = P(("sp", "tp"), None)
    return jax.shard_map(pick, mesh=mesh, in_specs=in_specs, out_specs=out_specs, check_vma=False)
```

profile of v0, /device:TPU:0, one launch (start us, length us, event | category | flops | bytes accessed | tf_op | source)
XLA Modules:
  0.0 136.1 jit_solution(10889516771861421209)
XLA Ops:
  0.0 1.3 reshape.3.refs_13_
  1.3 133.2 %fused.1 = bf16[32,2048]{1,0:T(8,128)(2,1)} custom-call(bf16[128,2048]{1,0:T(8,128)(2,1)} %refs_0_.1, bf16[128,256]{1,0:T(8,128)(2,1)} %refs_1_.1, bf16[128,256]{1,0:T(8,128)(2,1)} %refs_2_.1, bf16[128,256]{1,0:T(8,128)(2,1)} %refs_3_.1, bf16[128,256]{1,0:T(8,128)(2,1)} %refs_4_.1, f32[4,2,128]{2,1,0:T(2,128)} %refs_5_.1, bf16[128,256]{1,0:T(8,128)(2,1)} %refs_6_.1, ...), custom_call_target="tpu_custom_call" | custom-call | tf_op jit(solution)/shard_map/fused/pallas_call | solution.py:524
  134.5 1.6 %copy.19 = bf16[32,2048]{1,0:T(8,128)(2,1)} copy(bf16[32,2048]{1,0:T(8,128)(2,1)} %fused.1) | data formatting | bytes 262144
where the time goes:
time: 137 us; the launch traced here: 136 us
  Pallas kernels  133 us (97%)
  local copies, waits for them, and re-layouts  2.86 us (2%)
    pallas_call x1, Pallas kernels, fused_shards(): pl.pallas_call(functools.partial(fused_kernel, geometry), out_shape=jax.S...  133 us

commit v1 on v0

--- a/solution.py
+++ b/solution.py
@@ -12,6 +12,8 @@
 
 EPSILON = 1e-06
 FAR = -1e30
+LATE = 1
+SHARED = 1
 MESH = pl.DeviceIdType.MESH
 
 
@@ -134,26 +136,35 @@
 def fused_kernel(geometry, *refs):
     spread, members, wide, narrow_heads, broad_heads = geometry
     (res, qn, kn, vn, on, gn, qb, kb, vb, ob, gb, opn, opb, gain, gw, uw, dw, out) = refs[:18]
-    (kv_all, info, gates, wt, w_all, pp, rs, x_all, part, r1l, r1r, s1l, s1r, r2l, r2r, s2, r3) = (
-        refs[18:35]
-    )
-    (kv_send, kv_recv, in_send, in_recv, w_send, w_recv, f_send, f_recv) = refs[35:43]
-    (p_send, p_recv, x_send, x_recv, e_send, e_recv, z_send, z_recv) = refs[43:51]
+    (kv_all, info, gates, wt, w_all, pp, rs, x_all, part, r1, s2, r3) = refs[18:30]
+    (kv_send, kv_recv, in_send, in_recv, w_send, w_recv, f_send, f_recv, g_send, g_recv) = refs[30:40]
+    (p_send, p_recv, x_send, x_recv, e_send, e_recv, z_send, z_recv) = refs[40:48]
     rows = res.shape[0]
     own = rows // members
-    depth, tall = spread // 2, members // 2
+    depth = spread // 2
     chan, hid = gw.shape
     piece = hid // spread
     ca, cb = kn.shape[1], kb.shape[1]
-    half = res.shape[1] // 2
     i, j = lax.axis_index("sp"), lax.axis_index("tp")
     z, x = i // 2, i % 2
     y, c = j // 2, j % 2
-    ox, oy = 1 - x, 1 - y
+    ox = 1 - x
     f32, bf16 = jnp.float32, jnp.bfloat16
-    pending = []
-
-    def send(src, dst, s_sem, r_sem, to, cond=None):
+    sibling, x_peer = (i, j + 1 - 2 * c), (2 * z + ox, j)
+    across = (1 - y) * 2 + c
+    y_peer = (i, across)
+
+    def ranked(n):
+        pick = 0
+        for a in range(depth):
+            others = sorted(
+                (b for b in range(depth) if b != a),
+                key=lambda b: (abs(a - b), (a < depth // 2) == (b < depth // 2)),
+            )
+            pick = pick + jnp.where(z == a, others[n], 0)
+        return pick
+
+    def send(src, dst, s_sem, r_sem, to):
         copy = pltpu.make_async_remote_copy(
             src_ref=src, dst_ref=dst, send_sem=s_sem, recv_sem=r_sem, device_id=to, device_id_type=MESH
         )
@@ -232,9 +243,30 @@
         for k in range(hid // 128):
             wt[m, k * 128 : (k + 1) * 128, :] = ref[:, k * 128 : (k + 1) * 128].T
     mine = pl.ds(pl.multiple_of(i * piece, 16), piece)
+
+    def w_slot(jj, p):
+        return w_all.at[:, jj, :, pl.ds(pl.multiple_of(p * chan, 128), chan)]
+
+    def send_weights(p):
+        theirs = pl.ds(pl.multiple_of(p * piece, 16), piece)
+        send(wt.at[:, theirs, :], w_slot(j, i), w_send.at[p], w_recv.at[i], (p, j))
+
+    def share_weights(p):
+        slot = w_slot(j, p)
+        arrived(slot, w_recv.at[p])
+        send(slot, slot, f_send.at[0, p], f_recv.at[0, p], sibling)
+        send(slot, slot, g_send.at[p], g_recv.at[p], y_peer)
+
+    def share_across(p):
+        slot = w_slot(across, p)
+        arrived(slot, g_recv.at[p])
+        send(slot, slot, f_send.at[1, p], f_recv.at[1, p], sibling)
+
     columns = pl.ds(pl.multiple_of(i * chan, 128), chan)
-    w_all[:, c, :, columns] = wt[:, mine, :]
-
+    block = wt.at[:, mine, :]
+    send(block, w_slot(j, i), g_send.at[i], g_recv.at[i], y_peer)
+    send(block, w_slot(j, i), f_send.at[0, i], f_recv.at[0, i], sibling)
+    w_all[:, j, :, columns] = wt[:, mine, :]
     for s in range(1, depth):
 
         @pl.when(z - s >= 0)
@@ -259,21 +291,32 @@
 
             pass_kv(slot, 2, (2 * z + ox, j))
 
-    sibling = (i, j + 1 - 2 * c)
-    send(wt.at[:, mine, :], w_all.at[:, c, :, columns], f_send.at[i], f_recv.at[i], sibling)
-    order = list(range(1, spread, 2)) + list(range(2, spread, 2))
-    early = len(order) - len(order) // 3
-
-    def send_weights(k):
-        p = (i + k) % spread
-        theirs = pl.ds(pl.multiple_of(p * piece, 16), piece)
-        send(wt.at[:, theirs, :], w_all.at[:, c, :, columns], w_send.at[p], w_recv.at[i], (p, j))
-
-    for k in order[:early]:
-        send_weights(k)
-
+    straight = [2 * ranked(n) + x for n in range(depth - 1)]
+    crossed = [2 * z + ox] + [2 * ranked(n) + ox for n in range(depth - 1)]
+    middle = jnp.logical_or(z == depth // 2 - 1, z == depth // 2)
+
+    @pl.when(middle)
+    def _():
+        send_weights(straight[0])
+
+    def kv_sent(slot, way, cond=None):
+        sent(kv_all.at[slot], kv_send.at[way, slot], cond)
+        sent(info.at[slot], in_send.at[way, slot], cond)
+
+    for zz in range(depth):
+        kv_sent(2 * zz + x, 0, jnp.logical_and(zz <= z, z + 1 < depth))
+        kv_sent(2 * zz + x, 1, jnp.logical_and(zz >= z, z >= 1))
+
+    @pl.when(jnp.logical_not(middle))
+    def _():
+        send_weights(straight[0])
+
+    for p in straight[1:]:
+        send_weights(p)
     for zz in range(depth):
         kv_arrived(2 * zz + ox)
+    for p in crossed[:LATE]:
+        send_weights(p)
 
     offset = jnp.zeros_like(total)
     pieces = [None] * spread
@@ -329,156 +372,117 @@
     for k in range(1, members):
         q = (j + k) % members
         send(pp.at[q], rs.at[j], p_send.at[q], p_recv.at[j], (i, q))
+    for p in straight[:SHARED]:
+        share_weights(p)
     stream = res[pl.ds(pl.multiple_of(j * own, own), own), :].astype(f32) + pp[j].astype(f32)
     for k in range(1, members):
         q = (j + k) % members
         arrived(rs.at[q], p_recv.at[q])
         stream = stream + rs[q].astype(f32)
     scaled = stream * lax.rsqrt(jnp.mean(stream * stream, axis=1, keepdims=True) + EPSILON)
-    x_all[x, y, z] = (scaled * gain[...].astype(f32)).astype(bf16)
-
-    def pass_x(xx, yy, zz, way, to):
-        slot = x_all.at[xx, yy, zz]
-        send(slot, slot, x_send.at[way, xx, yy, zz], x_recv.at[xx, yy, zz], to)
-
-    def x_arrived(xx, yy, zz):
-        arrived(x_all.at[xx, yy, zz], x_recv.at[xx, yy, zz])
-
-    x_peer, y_peer = (2 * z + ox, j), (i, 2 * oy + c)
+    x_all[x, z] = (scaled * gain[...].astype(f32).reshape(1, wide)).astype(bf16)
+
+    def pass_x(zz, way, to):
+        slot = x_all.at[x, zz]
+        send(slot, slot, x_send.at[way, zz], x_recv.at[x, zz], to)
+
+    def x_arrived(xx, zz):
+        arrived(x_all.at[xx, zz], x_recv.at[xx, zz])
 
     @pl.when(z + 1 < depth)
     def _():
-        pass_x(x, y, z, 0, (i + 2, j))
+        pass_x(z, 0, (i + 2, j))
 
     @pl.when(z >= 1)
     def _():
-        pass_x(x, y, z, 1, (i - 2, j))
-
-    pass_x(x, y, z, 2, x_peer)
-    pass_x(x, y, z, 3, y_peer)
+        pass_x(z, 1, (i - 2, j))
+
+    pass_x(z, 2, x_peer)
+    for p in crossed[LATE:]:
+        send_weights(p)
     for s in range(1, depth):
 
         @pl.when(z - s >= 0)
         def _():
-            x_arrived(x, y, z - s)
+            x_arrived(x, z - s)
 
             @pl.when(z + 1 < depth)
             def _():
-                pass_x(x, y, z - s, 0, (i + 2, j))
-
-            pass_x(x, y, z - s, 2, x_peer)
-            pass_x(x, y, z - s, 3, y_peer)
+                pass_x(z - s, 0, (i + 2, j))
+
+            pass_x(z - s, 2, x_peer)
 
         @pl.when(z + s < depth)
         def _():
-            x_arrived(x, y, z + s)
+            x_arrived(x, z + s)
 
             @pl.when(z >= 1)
             def _():
-                pass_x(x, y, z + s, 1, (i - 2, j))
-
-            pass_x(x, y, z + s, 2, x_peer)
-            pass_x(x, y, z + s, 3, y_peer)
-
-    for k in order[early:]:
-        send_weights(k)
-
+                pass_x(z + s, 1, (i - 2, j))
+
+            pass_x(z + s, 2, x_peer)
+
+    for p in straight[SHARED:] + crossed:
+        share_weights(p)
+    for p in [i] + straight + crossed:
+        share_across(p)
     for zz in range(depth):
-        x_arrived(x, oy, zz)
-        if zz < depth // 2:
-            pass_x(x, oy, zz, 2, x_peer)
-        x_arrived(ox, y, zz)
-        if zz >= depth // 2:
-            pass_x(ox, y, zz, 3, y_peer)
-
-    for k in order:
-        p = (i + spread - k) % spread
-        theirs = pl.ds(pl.multiple_of(p * chan, 128), chan)
-        slot = w_all.at[:, c, :, theirs]
-        arrived(slot, w_recv.at[p])
-        send(slot, slot, f_send.at[p], f_recv.at[p], sibling)
-    for k in [0] + order:
-        p = (i + spread - k) % spread
-        theirs = pl.ds(pl.multiple_of(p * chan, 128), chan)
-        arrived(w_all.at[:, 1 - c, :, theirs], f_recv.at[p])
-
-    units = 2 * piece
-
-    def chunk(xx, yy):
-        a = x_all[xx, yy].reshape(depth * own, -1)
+        x_arrived(ox, zz)
+    other, other_across = 2 * y + 1 - c, 2 * (1 - y) + 1 - c
+    for p in [i] + straight + crossed:
+        arrived(w_slot(other, p), f_recv.at[0, p])
+        arrived(w_slot(other_across, p), f_recv.at[1, p])
+
+    units = members * piece
+
+    def chunk(xx):
+        a = x_all[xx].reshape(depth * own, -1)
         gate = lax.dot_general(a, w_all[0].reshape(units, -1), nt, preferred_element_type=f32)
         up = lax.dot_general(a, w_all[1].reshape(units, -1), nt, preferred_element_type=f32)
         hidden = (gate / (1.0 + jnp.exp(-gate)) * up).astype(bf16)
         got = jnp.dot(hidden, w_all[2].reshape(units, -1), preferred_element_type=f32)
-        part[xx, yy] = got.astype(bf16).reshape(depth, own, -1)
-
-    left, right = slice(0, half), slice(half, 2 * half)
-    chunk(ox, y)
-    for zz in range(depth):
-        x_arrived(ox, oy, zz)
-    chunk(ox, oy)
-    send(part.at[ox, :, :, :, pl.ds(0, half)], r1l, e_send.at[0], e_recv.at[0], x_peer)
-    chunk(x, oy)
-    send(part.at[:, oy, :, :, pl.ds(half, half)], r1r, e_send.at[1], e_recv.at[1], y_peer)
-    chunk(x, y)
-    arrived(r1l, e_recv.at[0])
-    s1l[...] = (part[x, :, :, :, left].astype(f32) + r1l[...].astype(f32)).astype(bf16)
-    send(s1l.at[oy], r2l, e_send.at[2], e_recv.at[2], y_peer)
-    arrived(r1r, e_recv.at[1])
-    s1r[...] = (part[:, y, :, :, right].astype(f32) + r1r[...].astype(f32)).astype(bf16)
-    send(s1r.at[ox], r2r, e_send.at[3], e_recv.at[3], x_peer)
-    arrived(r2l, e_recv.at[2])
-    s2[:, :, left] = (s1l[y].astype(f32) + r2l[...].astype(f32)).astype(bf16)
-    arrived(r2r, e_recv.at[3])
-    s2[:, :, right] = (s1r[x].astype(f32) + r2r[...].astype(f32)).astype(bf16)
-    for k in range(1, depth):
-        zz = (z + k) % depth
+        part[xx] = got.astype(bf16).reshape(depth, own, -1)
+
+    ends = [(z + depth // 2) % depth] + [(z + k) % depth for k in range(1, depth) if 2 * k != depth]
+    chunk(ox)
+    for zz in ends + [z]:
+        send(part.at[ox, zz], r1.at[zz], e_send.at[zz], e_recv.at[zz], x_peer)
+    chunk(x)
+    for zz in ends:
+        arrived(r1.at[zz], e_recv.at[zz])
+        s2[zz] = (part[x, zz].astype(f32) + r1[zz].astype(f32)).astype(bf16)
         send(s2.at[zz], r3.at[z], z_send.at[zz], z_recv.at[z], (2 * zz + x, j))
-    ffn = s2[z].astype(f32)
-    for k in range(1, depth):
-        zz = (z + k) % depth
+    arrived(r1.at[z], e_recv.at[z])
+    ffn = part[x, z].astype(f32) + r1[z].astype(f32)
+    for zz in ends:
         arrived(r3.at[zz], z_recv.at[zz])
         ffn = ffn + r3[zz].astype(f32)
     out[...] = (stream + 0.5 * ffn).astype(out.dtype)
 
-    def kv_sent(slot, way, cond=None):
-        sent(kv_all.at[slot], kv_send.at[way, slot], cond)
-        sent(info.at[slot], in_send.at[way, slot], cond)
-
     for zz in range(depth):
-        kv_sent(2 * zz + x, 0, jnp.logical_and(zz <= z, z + 1 < depth))
-        kv_sent(2 * zz + x, 1, jnp.logical_and(zz >= z, z >= 1))
         kv_sent(2 * zz + x, 2)
-        slot = x_all.at[x, y, zz]
-        sent(slot, x_send.at[0, x, y, zz], jnp.logical_and(zz <= z, z + 1 < depth))
-        sent(slot, x_send.at[1, x, y, zz], jnp.logical_and(zz >= z, z >= 1))
-        sent(slot, x_send.at[2, x, y, zz])
-        sent(slot, x_send.at[3, x, y, zz])
-        if zz < depth // 2:
-            sent(slot, x_send.at[2, x, oy, zz])
-        else:
-            sent(slot, x_send.at[3, ox, y, zz])
-    block = wt.at[:, mine, :]
-    sent(block, f_send.at[i])
-    for k in range(1, spread):
-        p = (i + k) % spread
+        slot = x_all.at[x, zz]
+        sent(slot, x_send.at[0, zz], jnp.logical_and(zz <= z, z + 1 < depth))
+        sent(slot, x_send.at[1, zz], jnp.logical_and(zz >= z, z >= 1))
+        sent(slot, x_send.at[2, zz])
+        sent(r1.at[0], e_send.at[zz])
+    for p in straight + crossed:
         sent(block, w_send.at[p])
-        sent(block, f_send.at[p])
+    for p in range(spread):
+        sent(block, f_send.at[0, p])
+        sent(block, f_send.at[1, p])
+        sent(block, g_send.at[p])
     for k in range(1, members):
         sent(rs.at[0], p_send.at[(j + k) % members])
-    sent(r1l, e_send.at[0])
-    sent(r1r, e_send.at[1])
-    sent(r2l, e_send.at[2])
-    sent(r2r, e_send.at[3])
-    for k in range(1, depth):
-        sent(r3.at[0], z_send.at[(z + k) % depth])
+    for zz in ends:
+        sent(s2.at[0], z_send.at[zz])
 
 
 def fused_shards(*args):
     (res, qn, kn, vn, on, gn, qb, kb, vb, ob, gb, opn, opb, gain, gw, uw, dw) = args
     spread, members = lax.axis_size("sp"), lax.axis_size("tp")
     rows, wide = res.shape
-    own, depth, tall = rows // members, spread // 2, members // 2
+    own, depth = rows // members, spread // 2
     chan, hid = gw.shape
     piece = hid // spread
     kvw = 2 * (kn.shape[1] + kb.shape[1])
@@ -490,17 +494,12 @@
         v((spread, 2, 16, rows), f32),
         v((2, 16, rows), f32),
         v((3, hid, chan), bf16),
-        v((3, 2, piece, wide), bf16),
+        v((3, members, piece, wide), bf16),
         v((members, own, wide), bf16),
         v((members, own, wide), bf16),
-        v((2, tall, depth, own, wide), bf16),
-        v((2, tall, depth, own, wide), bf16),
-        v((tall, depth, own, wide // 2), bf16),
-        v((2, depth, own, wide // 2), bf16),
-        v((tall, depth, own, wide // 2), bf16),
-        v((2, depth, own, wide // 2), bf16),
-        v((depth, own, wide // 2), bf16),
-        v((depth, own, wide // 2), bf16),
+        v((2, depth, own, wide), bf16),
+        v((2, depth, own, wide), bf16),
+        v((depth, own, wide), bf16),
         v((depth, own, wide), bf16),
         v((depth, own, wide), bf16),
         dma((3, spread)),
@@ -509,14 +508,16 @@
         dma((spread,)),
         dma((spread,)),
         dma((spread,)),
+        dma((2, spread)),
+        dma((2, spread)),
         dma((spread,)),
         dma((spread,)),
         dma((members,)),
         dma((members,)),
-        dma((4, 2, tall, depth)),
-        dma((2, tall, depth)),
-        dma((4,)),
-        dma((4,)),
+        dma((3, depth)),
+        dma((2, depth)),
+        dma((depth,)),
+        dma((depth,)),
         dma((depth,)),
         dma((depth,)),
     ]
@@ -531,7 +532,7 @@
             collective_id=0, has_side_effects=True, vmem_limit_bytes=60 * 1024 * 1024
         ),
         name="fused",
-    )(res, qn, kn, vn, on, gn, qb, kb, vb, ob, gb, opn, opb, gain.reshape(1, -1), gw, uw, dw)
+    )(res, qn, kn, vn, on, gn, qb, kb, vb, ob, gb, opn, opb, gain, gw, uw, dw)
 
 
 def pick(*args):

time: 137 us -> 142 us (1.036)
  Pallas kernels: 133 us -> 138 us
    pallas_call x1, Pallas kernels: 133 us -> 138 us  [fused_shards(): pl.pallas_call(functools.partial(fused_kernel, geometry), out_shape=jax.S...]
where the time goes in v1:
time: 142 us; the launch traced here: 140 us
  Pallas kernels  138 us (97%)
  local copies, waits for them, and re-layouts  1.57 us (1%)
    pallas_call x1, Pallas kernels, fused_shards(): pl.pallas_call(functools.partial(fused_kernel, geometry), out_shape=jax.S...  138 us

profile of v1, /device:TPU:0, one launch (start us, length us, event | category | flops | bytes accessed | tf_op | source)
XLA Modules:
  0.0 139.7 jit_solution(1714849600637795426)
XLA Ops:
  0.0 138.2 %fused.1 = bf16[32,2048]{1,0:T(8,128)(2,1)} custom-call(bf16[128,2048]{1,0:T(8,128)(2,1)} %refs_0_.1, bf16[128,256]{1,0:T(8,128)(2,1)} %refs_1_.1, bf16[128,256]{1,0:T(8,128)(2,1)} %refs_2_.1, bf16[128,256]{1,0:T(8,128)(2,1)} %refs_3_.1, bf16[128,256]{1,0:T(8,128)(2,1)} %refs_4_.1, f32[4,2,128]{2,1,0:T(2,128)} %refs_5_.1, bf16[128,256]{1,0:T(8,128)(2,1)} %refs_6_.1, ...), custom_call_target="tpu_custom_call" | custom-call | tf_op jit(solution)/shard_map/fused/pallas_call | solution.py:525
  138.2 1.6 %copy.19 = bf16[32,2048]{1,0:T(8,128)(2,1)} copy(bf16[32,2048]{1,0:T(8,128)(2,1)} %fused.1) | data formatting | bytes 262144

commit v2 on v1

--- a/solution.py
+++ b/solution.py
@@ -12,8 +12,6 @@
 
 EPSILON = 1e-06
 FAR = -1e30
-LATE = 1
-SHARED = 1
 MESH = pl.DeviceIdType.MESH
 
 
@@ -311,11 +309,11 @@
     def _():
         send_weights(straight[0])
 
-    for p in straight[1:]:
-        send_weights(p)
+    send_weights(straight[1])
     for zz in range(depth):
         kv_arrived(2 * zz + ox)
-    for p in crossed[:LATE]:
+    send_weights(crossed[0])
+    for p in straight[2:]:
         send_weights(p)
 
     offset = jnp.zeros_like(total)
@@ -372,8 +370,9 @@
     for k in range(1, members):
         q = (j + k) % members
         send(pp.at[q], rs.at[j], p_send.at[q], p_recv.at[j], (i, q))
-    for p in straight[:SHARED]:
-        share_weights(p)
+    share_weights(straight[0])
+    for p in crossed[1:4]:
+        send_weights(p)
     stream = res[pl.ds(pl.multiple_of(j * own, own), own), :].astype(f32) + pp[j].astype(f32)
     for k in range(1, members):
         q = (j + k) % members
@@ -382,50 +381,39 @@
     scaled = stream * lax.rsqrt(jnp.mean(stream * stream, axis=1, keepdims=True) + EPSILON)
     x_all[x, z] = (scaled * gain[...].astype(f32).reshape(1, wide)).astype(bf16)
 
-    def pass_x(zz, way, to):
+    def pass_x(zz, sem, to):
         slot = x_all.at[x, zz]
-        send(slot, slot, x_send.at[way, zz], x_recv.at[x, zz], to)
+        send(slot, slot, sem, x_recv.at[x, zz], to)
 
     def x_arrived(xx, zz):
         arrived(x_all.at[xx, zz], x_recv.at[xx, zz])
 
-    @pl.when(z + 1 < depth)
-    def _():
-        pass_x(z, 0, (i + 2, j))
-
-    @pl.when(z >= 1)
-    def _():
-        pass_x(z, 1, (i - 2, j))
-
-    pass_x(z, 2, x_peer)
-    for p in crossed[LATE:]:
-        send_weights(p)
-    for s in range(1, depth):
-
-        @pl.when(z - s >= 0)
-        def _():
-            x_arrived(x, z - s)
-
-            @pl.when(z + 1 < depth)
-            def _():
-                pass_x(z - s, 0, (i + 2, j))
-
-            pass_x(z - s, 2, x_peer)
-
-        @pl.when(z + s < depth)
-        def _():
-            x_arrived(x, z + s)
-
-            @pl.when(z >= 1)
-            def _():
-                pass_x(z + s, 1, (i - 2, j))
-
-            pass_x(z + s, 2, x_peer)
-
-    for p in straight[SHARED:] + crossed:
-        share_weights(p)
-    for p in [i] + straight + crossed:
-        share_across(p)
+    for n in range(depth - 1):
+        pass_x(z, x_send.at[0, n], (2 * ranked(n) + x, j))
+    pass_x(z, x_send.at[1, z], x_peer)
+
+    def forward_x(n):
+        zz = ranked(n)
+        x_arrived(x, zz)
+        pass_x(zz, x_send.at[1, zz], x_peer)
+
+    share_weights(straight[1])
+    share_across(i)
+    share_weights(straight[2])
+    share_across(straight[0])
+    share_weights(crossed[0])
+    share_across(straight[1])
+    share_weights(crossed[1])
+    share_across(straight[2])
+    share_weights(crossed[2])
+    share_across(crossed[0])
+    share_weights(crossed[3])
+    forward_x(0)
+    forward_x(1)
+    forward_x(2)
+    share_across(crossed[1])
+    share_across(crossed[2])
+    share_across(crossed[3])
     for zz in range(depth):
         x_arrived(ox, zz)
     other, other_across = 2 * y + 1 - c, 2 * (1 - y) + 1 - c
@@ -462,10 +450,10 @@
     for zz in range(depth):
         kv_sent(2 * zz + x, 2)
         slot = x_all.at[x, zz]
-        sent(slot, x_send.at[0, zz], jnp.logical_and(zz <= z, z + 1 < depth))
-        sent(slot, x_send.at[1, zz], jnp.logical_and(zz >= z, z >= 1))
-        sent(slot, x_send.at[2, zz])
+        sent(slot, x_send.at[1, zz])
         sent(r1.at[0], e_send.at[zz])
+    for n in range(depth - 1):
+        sent(x_all.at[0, 0], x_send.at[0, n])
     for p in straight + crossed:
         sent(block, w_send.at[p])
     for p in range(spread):
@@ -514,7 +502,7 @@
         dma((spread,)),
         dma((members,)),
         dma((members,)),
-        dma((3, depth)),
+        dma((2, depth)),
         dma((2, depth)),
         dma((depth,)),
         dma((depth,)),

time: 142 us -> 115 us (0.81); the launches traced: 140 us -> 114 us
  Pallas kernels: 138 us -> 113 us
    pallas_call x1, Pallas kernels: 138 us -> 113 us  [fused_shards(): pl.pallas_call(functools.partial(fused_kernel, geometry), out_shape=jax.S...]
where the time goes in v2:
time: 115 us; the launch traced here: 114 us
  Pallas kernels  113 us (98%)
  local copies, waits for them, and re-layouts  1.57 us (1%)
    pallas_call x1, Pallas kernels, fused_shards(): pl.pallas_call(functools.partial(fused_kernel, geometry), out_shape=jax.S...  113 us

profile of v2, /device:TPU:0, one launch (start us, length us, event | category | flops | bytes accessed | tf_op | source)
XLA Modules:
  0.0 114.4 jit_solution(14579342403488284504)
XLA Ops:
  0.0 112.8 %fused.1 = bf16[32,2048]{1,0:T(8,128)(2,1)} custom-call(bf16[128,2048]{1,0:T(8,128)(2,1)} %refs_0_.1, bf16[128,256]{1,0:T(8,128)(2,1)} %refs_1_.1, bf16[128,256]{1,0:T(8,128)(2,1)} %refs_2_.1, bf16[128,256]{1,0:T(8,128)(2,1)} %refs_3_.1, bf16[128,256]{1,0:T(8,128)(2,1)} %refs_4_.1, f32[4,2,128]{2,1,0:T(2,128)} %refs_5_.1, bf16[128,256]{1,0:T(8,128)(2,1)} %refs_6_.1, ...), custom_call_target="tpu_custom_call" | custom-call | tf_op jit(solution)/shard_map/fused/pallas_call | solution.py:513
  112.8 1.6 %copy.19 = bf16[32,2048]{1,0:T(8,128)(2,1)} copy(bf16[32,2048]{1,0:T(8,128)(2,1)} %fused.1) | data formatting | bytes 262144

commit v3 on v2

--- a/solution.py
+++ b/solution.py
@@ -135,8 +135,10 @@
     spread, members, wide, narrow_heads, broad_heads = geometry
     (res, qn, kn, vn, on, gn, qb, kb, vb, ob, gb, opn, opb, gain, gw, uw, dw, out) = refs[:18]
     (kv_all, info, gates, wt, w_all, pp, rs, x_all, part, r1, s2, r3) = refs[18:30]
-    (kv_send, kv_recv, in_send, in_recv, w_send, w_recv, f_send, f_recv, g_send, g_recv) = refs[30:40]
-    (p_send, p_recv, x_send, x_recv, e_send, e_recv, z_send, z_recv) = refs[40:48]
+    (st_out, sn_out, st_in, sn_in) = refs[30:34]
+    (kv_send, kv_recv, in_send, in_recv, w_send, w_recv, f_send, f_recv, g_send, g_recv) = refs[34:44]
+    (p_send, p_recv, x_send, x_recv, e_send, e_recv, z_send, z_recv) = refs[44:52]
+    (st_send, st_recv, sn_recv) = refs[52:55]
     rows = res.shape[0]
     own = rows // members
     depth = spread // 2
@@ -147,6 +149,8 @@
     z, x = i // 2, i % 2
     y, c = j // 2, j % 2
     ox = 1 - x
+    size = spread // 2
+    half, local = i // size, i % size
     f32, bf16 = jnp.float32, jnp.bfloat16
     sibling, x_peer = (i, j + 1 - 2 * c), (2 * z + ox, j)
     across = (1 - y) * 2 + c
@@ -191,10 +195,10 @@
     for k in range(1, members):
         pl.semaphore_signal(barrier, inc=1, device_id=(i, (j + k) % members), device_id_type=MESH)
 
-    kv_all[i, :, 0:ca] = kn[...]
-    kv_all[i, :, ca : 2 * ca] = vn[...]
-    kv_all[i, :, 2 * ca : 2 * ca + cb] = kb[...]
-    kv_all[i, :, 2 * ca + cb : 2 * ca + 2 * cb] = vb[...]
+    kv_all[local, :, 0:ca] = kn[...]
+    kv_all[local, :, ca : 2 * ca] = vn[...]
+    kv_all[local, :, 2 * ca : 2 * ca + cb] = kb[...]
+    kv_all[local, :, 2 * ca + cb : 2 * ca + 2 * cb] = vb[...]
     gates[...] = jnp.zeros_like(gates)
     for role in range(4):
         at = 8 * (role % 2)
@@ -215,27 +219,15 @@
         jnp.broadcast_to(cumulative[:, 0:1], in_gate.shape),
     )
     own_column = in_gate - cumulative
-    info[i, 0] = total + own_column
-    info[i, 1] = total
+    info[local, 0] = total + own_column
+    info[local, 1] = total
     pl.semaphore_wait(barrier, spread + members - 2)
 
-    def pass_kv(slot, way, to):
-        send(kv_all.at[slot], kv_all.at[slot], kv_send.at[way, slot], kv_recv.at[slot], to)
-        send(info.at[slot], info.at[slot], in_send.at[way, slot], in_recv.at[slot], to)
-
-    def kv_arrived(slot):
-        arrived(kv_all.at[slot], kv_recv.at[slot])
-        arrived(info.at[slot], in_recv.at[slot])
-
-    @pl.when(z + 1 < depth)
-    def _():
-        pass_kv(i, 0, (i + 2, j))
-
-    @pl.when(z >= 1)
-    def _():
-        pass_kv(i, 1, (i - 2, j))
-
-    pass_kv(i, 2, (2 * z + ox, j))
+    mates = [(local + k) % size for k in range(1, size)]
+    for k, mate in enumerate(mates):
+        to = (half * size + mate, j)
+        send(kv_all.at[local], kv_all.at[local], kv_send.at[k], kv_recv.at[local], to)
+        send(info.at[local], info.at[local], in_send.at[k], in_recv.at[local], to)
 
     for m, ref in enumerate((gw, uw, dw)):
         for k in range(hid // 128):
@@ -265,75 +257,109 @@
     send(block, w_slot(j, i), g_send.at[i], g_recv.at[i], y_peer)
     send(block, w_slot(j, i), f_send.at[0, i], f_recv.at[0, i], sibling)
     w_all[:, j, :, columns] = wt[:, mine, :]
-    for s in range(1, depth):
-
-        @pl.when(z - s >= 0)
-        def _():
-            slot = i - 2 * s
-            kv_arrived(slot)
-
-            @pl.when(z + 1 < depth)
-            def _():
-                pass_kv(slot, 0, (i + 2, j))
-
-            pass_kv(slot, 2, (2 * z + ox, j))
-
-        @pl.when(z + s < depth)
-        def _():
-            slot = i + 2 * s
-            kv_arrived(slot)
-
-            @pl.when(z >= 1)
-            def _():
-                pass_kv(slot, 1, (i - 2, j))
-
-            pass_kv(slot, 2, (2 * z + ox, j))
-
     straight = [2 * ranked(n) + x for n in range(depth - 1)]
     crossed = [2 * z + ox] + [2 * ranked(n) + ox for n in range(depth - 1)]
     middle = jnp.logical_or(z == depth // 2 - 1, z == depth // 2)
 
     @pl.when(middle)
     def _():
-        send_weights(straight[0])
-
-    def kv_sent(slot, way, cond=None):
-        sent(kv_all.at[slot], kv_send.at[way, slot], cond)
-        sent(info.at[slot], in_send.at[way, slot], cond)
-
-    for zz in range(depth):
-        kv_sent(2 * zz + x, 0, jnp.logical_and(zz <= z, z + 1 < depth))
-        kv_sent(2 * zz + x, 1, jnp.logical_and(zz >= z, z >= 1))
+        for p in (straight[0], crossed[1], straight[2], straight[1]):
+            send_weights(p)
 
     @pl.when(jnp.logical_not(middle))
     def _():
-        send_weights(straight[0])
-
-    send_weights(straight[1])
-    for zz in range(depth):
-        kv_arrived(2 * zz + ox)
+        send_weights(straight[1])
+
     send_weights(crossed[0])
-    for p in straight[2:]:
-        send_weights(p)
-
-    offset = jnp.zeros_like(total)
-    pieces = [None] * spread
+    in_turn = [
+        jnp.where(middle, a, b)
+        for a, b in zip(
+            [straight[0], crossed[1], crossed[0], straight[2], crossed[3], straight[1], crossed[2]],
+            [straight[0], crossed[0], straight[1], crossed[1], crossed[2], straight[2], crossed[3]],
+        )
+    ]
+
+    for mate in mates:
+        arrived(kv_all.at[mate], kv_recv.at[mate])
+        arrived(info.at[mate], in_recv.at[mate])
+
+    before, after = [], [None] * size
+    passed = jnp.zeros_like(total)
+    for k in range(size):
+        before.append(passed)
+        passed = passed + info[k, 1]
+    passed = jnp.zeros_like(total)
+    for k in reversed(range(size)):
+        after[k] = passed
+        passed = passed + info[k, 1]
+    to_end = jnp.concatenate(
+        [info[k, 0] + jnp.where(forward_row, after[k], before[k]) for k in range(size)], axis=1
+    )
+    to_end = jnp.where(half == 0, to_end[0:8], to_end[8:16])
+    end_max = jnp.max(to_end, axis=1, keepdims=True)
+    share = jnp.transpose(
+        jnp.concatenate([jnp.exp(to_end - end_max), jnp.zeros((rows - 8, size * rows), f32)], axis=0)
+    )
+    share_a = jnp.where(x == 0, share[:, 0:1], share[:, 1:2])
+    share_b = share[:, narrow_heads : narrow_heads + 1]
+    wa, wb = ca // narrow_heads, cb // 2
+
+    def kv_lanes(start, width):
+        return kv_all[:, :, pl.ds(pl.multiple_of(start, 128), width)].reshape(size * rows, width)
+
+    tn = (((0,), (0,)), ((), ()))
+    keys_a, keys_b = kv_lanes(x * wa, wa), kv_lanes(2 * ca, cb)
+    values_a = (share_a * kv_lanes(ca + x * wa, wa).astype(f32)).astype(bf16)
+    values_b = (share_b * kv_lanes(2 * ca + cb + x * wb, wb).astype(f32)).astype(bf16)
+    st_out[0:wa, :] = lax.dot_general(keys_a, values_a, tn, preferred_element_type=f32).astype(bf16)
+    st_out[wa : wa + cb, :] = lax.dot_general(keys_b, values_b, tn, preferred_element_type=f32).astype(bf16)
+    norm_a = jnp.sum(share_a * keys_a.astype(f32), axis=0, keepdims=True)
+    norm_b = jnp.sum(share_b * keys_b.astype(f32), axis=0, keepdims=True)
+    sn_out[:, 0:wa] = jnp.broadcast_to(norm_a, (8, wa))
+    sn_out[:, wa : wa + cb] = jnp.broadcast_to(norm_b, (8, cb))
+    sn_out[:, wa + cb :] = jnp.broadcast_to(end_max, (8, rows))
+    mirror = ((i + size) % spread, j)
+    send(sn_out, sn_in.at[x], st_send.at[1], sn_recv.at[x], mirror)
+    send(st_out, st_in.at[x], st_send.at[0], st_recv.at[x], mirror)
+
+    @pl.when(middle)
+    def _():
+        for p in (crossed[3], crossed[2]):
+            send_weights(p)
+
+    @pl.when(jnp.logical_not(middle))
+    def _():
+        for p in (straight[2], crossed[2], straight[0], crossed[3], crossed[1]):
+            send_weights(p)
+
+    for p in in_turn[:3]:
+        share_weights(p)
+    arrived(sn_in.at[x], sn_recv.at[x])
+    arrived(st_in.at[x], st_recv.at[x])
+    send(sn_in.at[x], sn_in.at[x], st_send.at[3], sn_recv.at[x], x_peer)
+    send(st_in.at[x], st_in.at[x], st_send.at[2], st_recv.at[x], x_peer)
+    arrived(sn_in.at[ox], sn_recv.at[ox])
+    arrived(st_in.at[ox], st_recv.at[ox])
+
+    pieces = [None] * size
     forward_sum = jnp.zeros_like(total)
-    ahead = [None] * spread
-    for k in reversed(range(spread)):
+    ahead = [None] * size
+    for k in reversed(range(size)):
         ahead[k] = forward_sum
-        forward_sum = forward_sum + jnp.where(k < i, info[k, 1], 0.0)
+        forward_sum = forward_sum + jnp.where(k < local, info[k, 1], 0.0)
     backward_sum = jnp.zeros_like(total)
-    for k in range(spread):
+    for k in range(size):
         reach = jnp.where(forward_row, ahead[k], backward_sum) + info[k, 0]
         seen = jnp.logical_or(
-            jnp.logical_and(forward_row, k < i), jnp.logical_and(jnp.logical_not(forward_row), k > i)
+            jnp.logical_and(forward_row, k < local),
+            jnp.logical_and(jnp.logical_not(forward_row), k > local),
         )
-        pieces[k] = jnp.where(k == i, own_column, jnp.where(seen, reach, FAR))
-        backward_sum = backward_sum + jnp.where(k > i, info[k, 1], 0.0)
+        pieces[k] = jnp.where(k == local, own_column, jnp.where(seen, reach, FAR))
+        backward_sum = backward_sum + jnp.where(k > local, info[k, 1], 0.0)
     column = jnp.concatenate(pieces, axis=1)
-    t_at = lax.broadcasted_iota(jnp.int32, (rows, spread * rows), 0) + i * rows
-    s_at = lax.broadcasted_iota(jnp.int32, (rows, spread * rows), 1)
+    past = sn_in[x, :, wa + cb :] + jnp.where(half == 1, forward_sum[0:8], backward_sum[8:16])
+    t_at = lax.broadcasted_iota(jnp.int32, (rows, size * rows), 0) + local * rows
+    s_at = lax.broadcasted_iota(jnp.int32, (rows, size * rows), 1)
     masks = (s_at <= t_at, s_at >= t_at)
     nt = (((1,), (1,)), ((), ()))
     proj = jnp.zeros((rows, res.shape[1]), f32)
@@ -343,11 +369,19 @@
     ]
     for query, outgate, outproj, base, group, h, width, row in heads:
         lanes = slice(h * width, (h + 1) * width)
-        keys = kv_all[:, :, base + h * width : base + (h + 1) * width].reshape(spread * rows, width)
+        keys = kv_all[:, :, base + h * width : base + (h + 1) * width].reshape(size * rows, width)
         vals = kv_all[:, :, base + group + h * width : base + group + (h + 1) * width].reshape(
-            spread * rows, width
+            size * rows, width
         )
-        scores = lax.dot_general(query[:, lanes], keys, nt, preferred_element_type=f32) * width ** (-0.5)
+        queries = query[:, lanes]
+        scores = lax.dot_general(queries, keys, nt, preferred_element_type=f32) * width ** (-0.5)
+        if row < narrow_heads:
+            memory, normer = st_in[row, 0:wa, :], sn_in[row, 0:1, 0:wa]
+        else:
+            memory = jnp.concatenate([st_in[0, wa:, :], st_in[1, wa:, :]], axis=1)
+            normer = sn_in[0, 0:1, wa : wa + cb]
+        recalled = jnp.dot(queries, memory, preferred_element_type=f32) * width ** (-0.5)
+        recall_den = jnp.sum(queries.astype(f32) * normer, axis=1, keepdims=True) * width ** (-0.5)
         summed = jnp.zeros((rows, width), f32)
         for direction in range(2):
             at = 8 * direction + row
@@ -356,10 +390,12 @@
                 jnp.broadcast_to(column[at : at + 1, :], scores.shape),
                 FAR,
             )
-            top = jnp.max(weight, axis=1, keepdims=True)
+            carried = jnp.where(half == 1 - direction, past[row : row + 1, 0:1], FAR)
+            top = jnp.maximum(jnp.max(weight, axis=1, keepdims=True), carried)
+            kept = jnp.exp(carried - top)
             p = jnp.exp(weight - top) * scores
-            den = jnp.sum(p, axis=1, keepdims=True)
-            num = jnp.dot(p.astype(bf16), vals, preferred_element_type=f32)
+            den = jnp.sum(p, axis=1, keepdims=True) + kept * recall_den
+            num = jnp.dot(p.astype(bf16), vals, preferred_element_type=f32) + kept * recalled
             summed = summed + num / jnp.maximum(jnp.abs(den), 1.0)
         normed = summed * lax.rsqrt(jnp.mean(summed * summed, axis=1, keepdims=True) + EPSILON)
         opened = 1.0 / (1.0 + jnp.exp(-outgate[:, lanes].astype(f32)))
@@ -370,9 +406,6 @@
     for k in range(1, members):
         q = (j + k) % members
         send(pp.at[q], rs.at[j], p_send.at[q], p_recv.at[j], (i, q))
-    share_weights(straight[0])
-    for p in crossed[1:4]:
-        send_weights(p)
     stream = res[pl.ds(pl.multiple_of(j * own, own), own), :].astype(f32) + pp[j].astype(f32)
     for k in range(1, members):
         q = (j + k) % members
@@ -397,27 +430,25 @@
         x_arrived(x, zz)
         pass_x(zz, x_send.at[1, zz], x_peer)
 
-    share_weights(straight[1])
+    share_weights(in_turn[3])
     share_across(i)
-    share_weights(straight[2])
-    share_across(straight[0])
-    share_weights(crossed[0])
-    share_across(straight[1])
-    share_weights(crossed[1])
-    share_across(straight[2])
-    share_weights(crossed[2])
-    share_across(crossed[0])
-    share_weights(crossed[3])
+    share_across(in_turn[0])
+    share_weights(in_turn[4])
+    share_across(in_turn[1])
+    share_across(in_turn[2])
+    share_weights(in_turn[5])
+    share_weights(in_turn[6])
+    share_across(in_turn[3])
     forward_x(0)
     forward_x(1)
     forward_x(2)
-    share_across(crossed[1])
-    share_across(crossed[2])
-    share_across(crossed[3])
+    share_across(in_turn[4])
+    share_across(in_turn[5])
+    share_across(in_turn[6])
     for zz in range(depth):
         x_arrived(ox, zz)
     other, other_across = 2 * y + 1 - c, 2 * (1 - y) + 1 - c
-    for p in [i] + straight + crossed:
+    for p in [i] + in_turn:
         arrived(w_slot(other, p), f_recv.at[0, p])
         arrived(w_slot(other_across, p), f_recv.at[1, p])
 
@@ -447,8 +478,14 @@
         ffn = ffn + r3[zz].astype(f32)
     out[...] = (stream + 0.5 * ffn).astype(out.dtype)
 
+    for k in range(size - 1):
+        sent(kv_all.at[0], kv_send.at[k])
+        sent(info.at[0], in_send.at[k])
+    sent(st_out, st_send.at[0])
+    sent(sn_out, st_send.at[1])
+    sent(st_out, st_send.at[2])
+    sent(sn_out, st_send.at[3])
     for zz in range(depth):
-        kv_sent(2 * zz + x, 2)
         slot = x_all.at[x, zz]
         sent(slot, x_send.at[1, zz])
         sent(r1.at[0], e_send.at[zz])
@@ -475,11 +512,12 @@
     piece = hid // spread
     kvw = 2 * (kn.shape[1] + kb.shape[1])
     bf16, f32 = jnp.bfloat16, jnp.float32
+    state_rows = DH_A + DH_B
     v = pltpu.VMEM
     dma = pltpu.SemaphoreType.DMA
     scratch = [
-        v((spread, rows, kvw), bf16),
-        v((spread, 2, 16, rows), f32),
+        v((spread // 2, rows, kvw), bf16),
+        v((spread // 2, 2, 16, rows), f32),
         v((2, 16, rows), f32),
         v((3, hid, chan), bf16),
         v((3, members, piece, wide), bf16),
@@ -490,10 +528,14 @@
         v((depth, own, wide), bf16),
         v((depth, own, wide), bf16),
         v((depth, own, wide), bf16),
-        dma((3, spread)),
-        dma((spread,)),
-        dma((3, spread)),
-        dma((spread,)),
+        v((state_rows, 128), bf16),
+        v((8, state_rows + rows), f32),
+        v((2, state_rows, 128), bf16),
+        v((2, 8, state_rows + rows), f32),
+        dma((spread // 2,)),
+        dma((spread // 2,)),
+        dma((spread // 2,)),
+        dma((spread // 2,)),
         dma((spread,)),
         dma((spread,)),
         dma((2, spread)),
@@ -508,6 +550,9 @@
         dma((depth,)),
         dma((depth,)),
         dma((depth,)),
+        dma((4,)),
+        dma((2,)),
+        dma((2,)),
     ]
     geometry = (spread, members, wide, gn.shape[1], gb.shape[1])
     return pl.pallas_call(
@@ -529,15 +574,17 @@
     rows = res.shape[0]
     chan, hid = gw.shape
     fits = (
-        spread % 2 == 0
-        and spread >= 4
+        spread == 8
         and members == 4
         and rows == 128
         and spread * rows <= 2048
         and chan % 128 == 0
         and hid % (16 * spread) == 0
         and hid % 128 == 0
-        and gn.shape[1] + gb.shape[1] <= 8
+        and (gn.shape[1], gb.shape[1]) == (2, 1)
+        and kn.shape[1] == 2 * DH_A
+        and DH_A == 128
+        and DH_B == 256
     )
     return fused_shards(*args) if fits else shards(*args)
 

time: 115 us -> 122 us (1.061)
  Pallas kernels: 113 us -> 121 us
    pallas_call x1, Pallas kernels: 113 us -> 121 us  [fused_shards(): pl.pallas_call(functools.partial(fused_kernel, geometry), out_shape=jax.S...]
where the time goes in v3:
time: 122 us
  Pallas kernels  121 us (99%)
  local copies, waits for them, and re-layouts  1.57 us (1%)
    pallas_call x1, Pallas kernels, fused_shards(): pl.pallas_call(functools.partial(fused_kernel, geometry), out_shape=jax.S...  121 us

profile of v3, /device:TPU:0, one launch (start us, length us, event | category | flops | bytes accessed | tf_op | source)
XLA Modules:
  0.0 122.2 jit_solution(16779791654343576791)
XLA Ops:
  0.0 120.6 %fused.1 = bf16[32,2048]{1,0:T(8,128)(2,1)} custom-call(bf16[128,2048]{1,0:T(8,128)(2,1)} %refs_0_.1, bf16[128,256]{1,0:T(8,128)(2,1)} %refs_1_.1, bf16[128,256]{1,0:T(8,128)(2,1)} %refs_2_.1, bf16[128,256]{1,0:T(8,128)(2,1)} %refs_3_.1, bf16[128,256]{1,0:T(8,128)(2,1)} %refs_4_.1, f32[4,2,128]{2,1,0:T(2,128)} %refs_5_.1, bf16[128,256]{1,0:T(8,128)(2,1)} %refs_6_.1, ...), custom_call_target="tpu_custom_call" | custom-call | tf_op jit(solution)/shard_map/fused/pallas_call | solution.py:558
  120.6 1.6 %copy.19 = bf16[32,2048]{1,0:T(8,128)(2,1)} copy(bf16[32,2048]{1,0:T(8,128)(2,1)} %fused.1) | data formatting | bytes 262144

commit v4 on v3

--- a/solution.py
+++ b/solution.py
@@ -263,7 +263,7 @@
 
     @pl.when(middle)
     def _():
-        for p in (straight[0], crossed[1], straight[2], straight[1]):
+        for p in (straight[2], straight[0], straight[1]):
             send_weights(p)
 
     @pl.when(jnp.logical_not(middle))
@@ -271,11 +271,16 @@
         send_weights(straight[1])
 
     send_weights(crossed[0])
+
+    @pl.when(middle)
+    def _():
+        send_weights(crossed[2])
+
     in_turn = [
         jnp.where(middle, a, b)
         for a, b in zip(
-            [straight[0], crossed[1], crossed[0], straight[2], crossed[3], straight[1], crossed[2]],
-            [straight[0], crossed[0], straight[1], crossed[1], crossed[2], straight[2], crossed[3]],
+            [straight[0], straight[2], crossed[0], straight[1], crossed[1], crossed[3], crossed[2]],
+            [straight[1], crossed[0], straight[0], crossed[1], straight[2], crossed[3], crossed[2]],
         )
     ]
 
@@ -324,20 +329,25 @@
 
     @pl.when(middle)
     def _():
-        for p in (crossed[3], crossed[2]):
+        for p in (crossed[1], crossed[3]):
             send_weights(p)
 
     @pl.when(jnp.logical_not(middle))
     def _():
-        for p in (straight[2], crossed[2], straight[0], crossed[3], crossed[1]):
-            send_weights(p)
-
-    for p in in_turn[:3]:
-        share_weights(p)
+        send_weights(straight[0])
+
+    share_weights(in_turn[0])
     arrived(sn_in.at[x], sn_recv.at[x])
     arrived(st_in.at[x], st_recv.at[x])
     send(sn_in.at[x], sn_in.at[x], st_send.at[3], sn_recv.at[x], x_peer)
     send(st_in.at[x], st_in.at[x], st_send.at[2], st_recv.at[x], x_peer)
+
+    @pl.when(jnp.logical_not(middle))
+    def _():
+        for p in (straight[2], crossed[2], crossed[3], crossed[1]):
+            send_weights(p)
+
+    share_weights(in_turn[1])
     arrived(sn_in.at[ox], sn_recv.at[ox])
     arrived(st_in.at[ox], st_recv.at[ox])
 
@@ -406,6 +416,7 @@
     for k in range(1, members):
         q = (j + k) % members
         send(pp.at[q], rs.at[j], p_send.at[q], p_recv.at[j], (i, q))
+    share_weights(in_turn[2])
     stream = res[pl.ds(pl.multiple_of(j * own, own), own), :].astype(f32) + pp[j].astype(f32)
     for k in range(1, members):
         q = (j + k) % members
@@ -435,8 +446,8 @@
     share_across(in_turn[0])
     share_weights(in_turn[4])
     share_across(in_turn[1])
+    share_weights(in_turn[5])
     share_across(in_turn[2])
-    share_weights(in_turn[5])
     share_weights(in_turn[6])
     share_across(in_turn[3])
     forward_x(0)

time: 122 us -> 102 us (0.84)
  Pallas kernels: 121 us -> 101 us
    pallas_call x1, Pallas kernels: 121 us -> 101 us  [fused_shards(): pl.pallas_call(functools.partial(fused_kernel, geometry), out_shape=jax.S...]
where the time goes in v4:
time: 102 us
  Pallas kernels  101 us (99%)
  local copies, waits for them, and re-layouts  1.57 us (2%)
    pallas_call x1, Pallas kernels, fused_shards(): pl.pallas_call(functools.partial(fused_kernel, geometry), out_shape=jax.S...  101 us

profile of v4, /device:TPU:0, one launch (start us, length us, event | category | flops | bytes accessed | tf_op | source)
XLA Modules:
  0.0 102.2 jit_solution(12025125551486983146)
XLA Ops:
  0.0 100.6 %fused.1 = bf16[32,2048]{1,0:T(8,128)(2,1)} custom-call(bf16[128,2048]{1,0:T(8,128)(2,1)} %refs_0_.1, bf16[128,256]{1,0:T(8,128)(2,1)} %refs_1_.1, bf16[128,256]{1,0:T(8,128)(2,1)} %refs_2_.1, bf16[128,256]{1,0:T(8,128)(2,1)} %refs_3_.1, bf16[128,256]{1,0:T(8,128)(2,1)} %refs_4_.1, f32[4,2,128]{2,1,0:T(2,128)} %refs_5_.1, bf16[128,256]{1,0:T(8,128)(2,1)} %refs_6_.1, ...), custom_call_target="tpu_custom_call" | custom-call | tf_op jit(solution)/shard_map/fused/pallas_call | solution.py:569
  100.6 1.6 %copy.19 = bf16[32,2048]{1,0:T(8,128)(2,1)} copy(bf16[32,2048]{1,0:T(8,128)(2,1)} %fused.1) | data formatting | bytes 262144

commit v5 on v4

--- a/solution.py
+++ b/solution.py
@@ -133,18 +133,19 @@
 
 def fused_kernel(geometry, *refs):
     spread, members, wide, narrow_heads, broad_heads = geometry
-    (res, qn, kn, vn, on, gn, qb, kb, vb, ob, gb, opn, opb, gain, gw, uw, dw, out) = refs[:18]
+    held, out = refs[:17], refs[17]
     (kv_all, info, gates, wt, w_all, pp, rs, x_all, part, r1, s2, r3) = refs[18:30]
     (st_out, sn_out, st_in, sn_in) = refs[30:34]
     (kv_send, kv_recv, in_send, in_recv, w_send, w_recv, f_send, f_recv, g_send, g_recv) = refs[34:44]
     (p_send, p_recv, x_send, x_recv, e_send, e_recv, z_send, z_recv) = refs[44:52]
-    (st_send, st_recv, sn_recv) = refs[52:55]
+    (st_send, st_recv, sn_recv, load_sem) = refs[52:56]
+    (res, qn, on, gn, qb, ob, gb, opn, opb, gain, gw, uw, dw) = refs[56:69]
     rows = res.shape[0]
     own = rows // members
     depth = spread // 2
     chan, hid = gw.shape
     piece = hid // spread
-    ca, cb = kn.shape[1], kb.shape[1]
+    ca, cb = held[2].shape[1], held[7].shape[1]
     i, j = lax.axis_index("sp"), lax.axis_index("tp")
     z, x = i // 2, i % 2
     y, c = j // 2, j % 2
@@ -195,10 +196,35 @@
     for k in range(1, members):
         pl.semaphore_signal(barrier, inc=1, device_id=(i, (j + k) % members), device_id_type=MESH)
 
-    kv_all[local, :, 0:ca] = kn[...]
-    kv_all[local, :, ca : 2 * ca] = vn[...]
-    kv_all[local, :, 2 * ca : 2 * ca + cb] = kb[...]
-    kv_all[local, :, 2 * ca + cb : 2 * ca + 2 * cb] = vb[...]
+    mine_kv = kv_all.at[local]
+    targets = {
+        5: gn,
+        10: gb,
+        2: mine_kv.at[:, 0:ca],
+        3: mine_kv.at[:, ca : 2 * ca],
+        7: mine_kv.at[:, 2 * ca : 2 * ca + cb],
+        8: mine_kv.at[:, 2 * ca + cb : 2 * ca + 2 * cb],
+        14: gw,
+        15: uw,
+        16: dw,
+        1: qn,
+        6: qb,
+        4: on,
+        9: ob,
+        11: opn,
+        12: opb,
+        0: res,
+        13: gain,
+    }
+    loads = {n: pltpu.make_async_copy(held[n], ref, load_sem.at[n]) for n, ref in targets.items()}
+    for load in loads.values():
+        load.start()
+
+    def loaded(*numbers):
+        for n in numbers:
+            loads[n].wait()
+
+    loaded(5, 10)
     gates[...] = jnp.zeros_like(gates)
     for role in range(4):
         at = 8 * (role % 2)
@@ -223,12 +249,14 @@
     info[local, 1] = total
     pl.semaphore_wait(barrier, spread + members - 2)
 
+    loaded(2, 3, 7, 8)
     mates = [(local + k) % size for k in range(1, size)]
     for k, mate in enumerate(mates):
         to = (half * size + mate, j)
         send(kv_all.at[local], kv_all.at[local], kv_send.at[k], kv_recv.at[local], to)
         send(info.at[local], info.at[local], in_send.at[k], in_recv.at[local], to)
 
+    loaded(14, 15, 16)
     for m, ref in enumerate((gw, uw, dw)):
         for k in range(hid // 128):
             wt[m, k * 128 : (k + 1) * 128, :] = ref[:, k * 128 : (k + 1) * 128].T
@@ -351,6 +379,7 @@
     arrived(sn_in.at[ox], sn_recv.at[ox])
     arrived(st_in.at[ox], st_recv.at[ox])
 
+    loaded(1, 6, 4, 9, 11, 12, 0, 13)
     pieces = [None] * size
     forward_sum = jnp.zeros_like(total)
     ahead = [None] * size
@@ -432,13 +461,19 @@
     def x_arrived(xx, zz):
         arrived(x_all.at[xx, zz], x_recv.at[xx, zz])
 
-    for n in range(depth - 1):
+    for n in range(2):
         pass_x(z, x_send.at[0, n], (2 * ranked(n) + x, j))
     pass_x(z, x_send.at[1, z], x_peer)
 
     def forward_x(n):
         zz = ranked(n)
         x_arrived(x, zz)
+        if n != 1:
+
+            @pl.when(middle)
+            def _():
+                pass_x(zz, x_send.at[0, 2 + n // 2], (2 * ranked(1) + x, j))
+
         pass_x(zz, x_send.at[1, zz], x_peer)
 
     share_weights(in_turn[3])
@@ -450,9 +485,9 @@
     share_across(in_turn[2])
     share_weights(in_turn[6])
     share_across(in_turn[3])
+    forward_x(2)
+    forward_x(1)
     forward_x(0)
-    forward_x(1)
-    forward_x(2)
     share_across(in_turn[4])
     share_across(in_turn[5])
     share_across(in_turn[6])
@@ -500,8 +535,8 @@
         slot = x_all.at[x, zz]
         sent(slot, x_send.at[1, zz])
         sent(r1.at[0], e_send.at[zz])
-    for n in range(depth - 1):
-        sent(x_all.at[0, 0], x_send.at[0, n])
+    for n in range(4):
+        sent(x_all.at[0, 0], x_send.at[0, n], None if n < 2 else middle)
     for p in straight + crossed:
         sent(block, w_send.at[p])
     for p in range(spread):
@@ -564,19 +599,21 @@
         dma((4,)),
         dma((2,)),
         dma((2,)),
+        dma((17,)),
     ]
+    scratch += [v(a.shape, a.dtype) for a in (res, qn, on, gn, qb, ob, gb, opn, opb, gain, gw, uw, dw)]
     geometry = (spread, members, wide, gn.shape[1], gb.shape[1])
     return pl.pallas_call(
         functools.partial(fused_kernel, geometry),
         out_shape=jax.ShapeDtypeStruct((own, wide), bf16),
-        in_specs=[pl.BlockSpec(memory_space=pltpu.VMEM)] * 17,
+        in_specs=[pl.BlockSpec(memory_space=pltpu.HBM)] * 17,
         out_specs=pl.BlockSpec(memory_space=pltpu.VMEM),
         scratch_shapes=scratch,
         compiler_params=pltpu.CompilerParams(
-            collective_id=0, has_side_effects=True, vmem_limit_bytes=60 * 1024 * 1024
+            collective_id=0, has_side_effects=True, vmem_limit_bytes=40 * 1024 * 1024
         ),
         name="fused",
-    )(res, qn, kn, vn, on, gn, qb, kb, vb, ob, gb, opn, opb, gain, gw, uw, dw)
+    )(*[pltpu.with_memory_space_constraint(a, pltpu.HBM) for a in args])
 
 
 def pick(*args):

time: 102 us -> 95.9 us (0.940)
  Pallas kernels: 101 us -> 95 us
    pallas_call x1, Pallas kernels: 101 us -> 95 us  [fused_shards(): pl.pallas_call(functools.partial(fused_kernel, geometry), out_shape=jax.S...]
where the time goes in v5:
time: 95.9 us; the launch traced here: 95.7 us
  Pallas kernels  95 us (99%)
    pallas_call x1, Pallas kernels, fused_shards(): pl.pallas_call(functools.partial(fused_kernel, geometry), out_shape=jax.S...  95 us

profile of v5, /device:TPU:0, one launch (start us, length us, event | category | flops | bytes accessed | tf_op | source)
XLA Modules:
  0.0 95.7 jit_solution(11186747101550141007)
XLA Ops:
  0.0 95.0 %fused.1 = bf16[32,2048]{1,0:T(8,128)(2,1)S(1)} custom-call(bf16[128,2048]{1,0:T(8,128)(2,1)} %refs_0_.1, bf16[128,256]{1,0:T(8,128)(2,1)} %refs_1_.1, bf16[128,256]{1,0:T(8,128)(2,1)} %refs_2_.1, bf16[128,256]{1,0:T(8,128)(2,1)} %refs_3_.1, bf16[128,256]{1,0:T(8,128)(2,1)} %refs_4_.1, f32[4,2,128]{2,1,0:T(2,128)} %refs_5_.1, bf16[128,256]{1,0:T(8,128)(2,1)} %refs_6_.1, ...), custom_call_target="tpu_custom_call" | custom-call | tf_op jit(solution)/shard_map/fused/pallas_call | solution.py:606
  95.0 0.7 copy.19

commit v6 on v5

--- a/solution.py
+++ b/solution.py
@@ -262,28 +262,32 @@
             wt[m, k * 128 : (k + 1) * 128, :] = ref[:, k * 128 : (k + 1) * 128].T
     mine = pl.ds(pl.multiple_of(i * piece, 16), piece)
 
-    def w_slot(jj, p):
-        return w_all.at[:, jj, :, pl.ds(pl.multiple_of(p * chan, 128), chan)]
-
-    def send_weights(p):
+    whole, first, last = (0, 0, 3), (0, 0, 2), (1, 2, 3)
+
+    def w_slot(jj, p, cut):
+        return w_all.at[cut[1] : cut[2], jj, :, pl.ds(pl.multiple_of(p * chan, 128), chan)]
+
+    def send_weights(p, part=whole):
         theirs = pl.ds(pl.multiple_of(p * piece, 16), piece)
-        send(wt.at[:, theirs, :], w_slot(j, i), w_send.at[p], w_recv.at[i], (p, j))
-
-    def share_weights(p):
-        slot = w_slot(j, p)
-        arrived(slot, w_recv.at[p])
-        send(slot, slot, f_send.at[0, p], f_recv.at[0, p], sibling)
-        send(slot, slot, g_send.at[p], g_recv.at[p], y_peer)
-
-    def share_across(p):
-        slot = w_slot(across, p)
-        arrived(slot, g_recv.at[p])
-        send(slot, slot, f_send.at[1, p], f_recv.at[1, p], sibling)
+        n = part[0]
+        source = wt.at[part[1] : part[2], theirs, :]
+        send(source, w_slot(j, i, part), w_send.at[n, p], w_recv.at[n, i], (p, j))
+
+    def share_weights(p, part=whole):
+        slot, n = w_slot(j, p, part), part[0]
+        arrived(slot, w_recv.at[n, p])
+        send(slot, slot, f_send.at[2 * n, p], f_recv.at[2 * n, p], sibling)
+        send(slot, slot, g_send.at[n, p], g_recv.at[n, p], y_peer)
+
+    def share_across(p, part=whole):
+        slot, n = w_slot(across, p, part), part[0]
+        arrived(slot, g_recv.at[n, p])
+        send(slot, slot, f_send.at[2 * n + 1, p], f_recv.at[2 * n + 1, p], sibling)
 
     columns = pl.ds(pl.multiple_of(i * chan, 128), chan)
     block = wt.at[:, mine, :]
-    send(block, w_slot(j, i), g_send.at[i], g_recv.at[i], y_peer)
-    send(block, w_slot(j, i), f_send.at[0, i], f_recv.at[0, i], sibling)
+    send(block, w_slot(j, i, whole), g_send.at[0, i], g_recv.at[0, i], y_peer)
+    send(block, w_slot(j, i, whole), f_send.at[0, i], f_recv.at[0, i], sibling)
     w_all[:, j, :, columns] = wt[:, mine, :]
     straight = [2 * ranked(n) + x for n in range(depth - 1)]
     crossed = [2 * z + ox] + [2 * ranked(n) + ox for n in range(depth - 1)]
@@ -302,13 +306,13 @@
 
     @pl.when(middle)
     def _():
-        send_weights(crossed[2])
+        send_weights(crossed[2], first)
 
     in_turn = [
         jnp.where(middle, a, b)
         for a, b in zip(
             [straight[0], straight[2], crossed[0], straight[1], crossed[1], crossed[3], crossed[2]],
-            [straight[1], crossed[0], straight[0], crossed[1], straight[2], crossed[3], crossed[2]],
+            [straight[1], crossed[0], straight[0], straight[2], crossed[1], crossed[3], crossed[2]],
         )
     ]
 
@@ -358,7 +362,7 @@
     @pl.when(middle)
     def _():
         for p in (crossed[1], crossed[3]):
-            send_weights(p)
+            send_weights(p, first)
 
     @pl.when(jnp.logical_not(middle))
     def _():
@@ -372,8 +376,9 @@
 
     @pl.when(jnp.logical_not(middle))
     def _():
-        for p in (straight[2], crossed[2], crossed[3], crossed[1]):
-            send_weights(p)
+        send_weights(straight[2])
+        for p in (crossed[2], crossed[3], crossed[1]):
+            send_weights(p, first)
 
     share_weights(in_turn[1])
     arrived(sn_in.at[ox], sn_recv.at[ox])
@@ -476,43 +481,54 @@
 
         pass_x(zz, x_send.at[1, zz], x_peer)
 
+    for p in (crossed[2], crossed[3], crossed[1]):
+        send_weights(p, last)
     share_weights(in_turn[3])
     share_across(i)
     share_across(in_turn[0])
-    share_weights(in_turn[4])
+    share_weights(in_turn[4], first)
     share_across(in_turn[1])
-    share_weights(in_turn[5])
+    share_weights(in_turn[5], first)
     share_across(in_turn[2])
-    share_weights(in_turn[6])
+    share_weights(in_turn[6], first)
     share_across(in_turn[3])
     forward_x(2)
     forward_x(1)
     forward_x(0)
-    share_across(in_turn[4])
-    share_across(in_turn[5])
-    share_across(in_turn[6])
+    for p in in_turn[4:]:
+        share_weights(p, last)
+    for p in in_turn[4:]:
+        share_across(p, first)
     for zz in range(depth):
         x_arrived(ox, zz)
+    for p in in_turn[4:]:
+        share_across(p, last)
     other, other_across = 2 * y + 1 - c, 2 * (1 - y) + 1 - c
-    for p in [i] + in_turn:
-        arrived(w_slot(other, p), f_recv.at[0, p])
-        arrived(w_slot(other_across, p), f_recv.at[1, p])
+    for p, cut in [(i, whole)] + [(p, whole) for p in in_turn[:4]] + [(p, first) for p in in_turn[4:]]:
+        arrived(w_slot(other, p, cut), f_recv.at[0, p])
+        arrived(w_slot(other_across, p, cut), f_recv.at[1, p])
 
     units = members * piece
 
-    def chunk(xx):
+    def hidden_of(xx):
         a = x_all[xx].reshape(depth * own, -1)
         gate = lax.dot_general(a, w_all[0].reshape(units, -1), nt, preferred_element_type=f32)
         up = lax.dot_general(a, w_all[1].reshape(units, -1), nt, preferred_element_type=f32)
-        hidden = (gate / (1.0 + jnp.exp(-gate)) * up).astype(bf16)
+        return (gate / (1.0 + jnp.exp(-gate)) * up).astype(bf16)
+
+    def project(xx, hidden):
         got = jnp.dot(hidden, w_all[2].reshape(units, -1), preferred_element_type=f32)
         part[xx] = got.astype(bf16).reshape(depth, own, -1)
 
     ends = [(z + depth // 2) % depth] + [(z + k) % depth for k in range(1, depth) if 2 * k != depth]
-    chunk(ox)
+    hidden = hidden_of(ox)
+    for p in in_turn[4:]:
+        arrived(w_slot(other, p, last), f_recv.at[2, p])
+        arrived(w_slot(other_across, p, last), f_recv.at[3, p])
+    project(ox, hidden)
     for zz in ends + [z]:
         send(part.at[ox, zz], r1.at[zz], e_send.at[zz], e_recv.at[zz], x_peer)
-    chunk(x)
+    project(x, hidden_of(x))
     for zz in ends:
         arrived(r1.at[zz], e_recv.at[zz])
         s2[zz] = (part[x, zz].astype(f32) + r1[zz].astype(f32)).astype(bf16)
@@ -537,12 +553,21 @@
         sent(r1.at[0], e_send.at[zz])
     for n in range(4):
         sent(x_all.at[0, 0], x_send.at[0, n], None if n < 2 else middle)
-    for p in straight + crossed:
-        sent(block, w_send.at[p])
-    for p in range(spread):
-        sent(block, f_send.at[0, p])
-        sent(block, f_send.at[1, p])
-        sent(block, g_send.at[p])
+    late = wt.at[2:3, mine, :]
+    early = wt.at[0:2, mine, :]
+    for p in straight + crossed[:1]:
+        sent(block, w_send.at[0, p])
+    for p in crossed[1:]:
+        sent(early, w_send.at[0, p])
+        sent(late, w_send.at[1, p])
+    for p in [i] + in_turn[:4]:
+        for ref in (g_send.at[0, p], f_send.at[0, p], f_send.at[1, p]):
+            sent(block, ref)
+    for p in in_turn[4:]:
+        for ref in (g_send.at[0, p], f_send.at[0, p], f_send.at[1, p]):
+            sent(early, ref)
+        for ref in (g_send.at[1, p], f_send.at[2, p], f_send.at[3, p]):
+            sent(late, ref)
     for k in range(1, members):
         sent(rs.at[0], p_send.at[(j + k) % members])
     for zz in ends:
@@ -582,12 +607,12 @@
         dma((spread // 2,)),
         dma((spread // 2,)),
         dma((spread // 2,)),
-        dma((spread,)),
-        dma((spread,)),
         dma((2, spread)),
         dma((2, spread)),
-        dma((spread,)),
-        dma((spread,)),
+        dma((4, spread)),
+        dma((4, spread)),
+        dma((2, spread)),
+        dma((2, spread)),
         dma((members,)),
         dma((members,)),
         dma((2, depth)),

time: 95.9 us -> 94.3 us (0.983)
  Pallas kernels: 95 us -> 93.5 us
    pallas_call x1, Pallas kernels: 95 us -> 93.5 us  [fused_shards(): pl.pallas_call(functools.partial(fused_kernel, geometry), out_shape=jax.S...]
where the time goes in v6:
time: 94.3 us; the launch traced here: 94.2 us
  Pallas kernels  93.5 us (99%)
    pallas_call x1, Pallas kernels, fused_shards(): pl.pallas_call(functools.partial(fused_kernel, geometry), out_shape=jax.S...  93.5 us

profile of v6, /device:TPU:0, one launch (start us, length us, event | category | flops | bytes accessed | tf_op | source)
XLA Modules:
  0.0 94.2 jit_solution(2804862489740387922)
XLA Ops:
  0.0 93.5 %fused.1 = bf16[32,2048]{1,0:T(8,128)(2,1)S(1)} custom-call(bf16[128,2048]{1,0:T(8,128)(2,1)} %refs_0_.1, bf16[128,256]{1,0:T(8,128)(2,1)} %refs_1_.1, bf16[128,256]{1,0:T(8,128)(2,1)} %refs_2_.1, bf16[128,256]{1,0:T(8,128)(2,1)} %refs_3_.1, bf16[128,256]{1,0:T(8,128)(2,1)} %refs_4_.1, f32[4,2,128]{2,1,0:T(2,128)} %refs_5_.1, bf16[128,256]{1,0:T(8,128)(2,1)} %refs_6_.1, ...), custom_call_target="tpu_custom_call" | custom-call | tf_op jit(solution)/shard_map/fused/pallas_call | solution.py:631
  93.5 0.7 copy.19

commit v7 on v6

--- a/solution.py
+++ b/solution.py
@@ -316,6 +316,7 @@
         )
     ]
 
+    share_weights(in_turn[0])
     for mate in mates:
         arrived(kv_all.at[mate], kv_recv.at[mate])
         arrived(info.at[mate], in_recv.at[mate])
@@ -352,9 +353,10 @@
     st_out[wa : wa + cb, :] = lax.dot_general(keys_b, values_b, tn, preferred_element_type=f32).astype(bf16)
     norm_a = jnp.sum(share_a * keys_a.astype(f32), axis=0, keepdims=True)
     norm_b = jnp.sum(share_b * keys_b.astype(f32), axis=0, keepdims=True)
-    sn_out[:, 0:wa] = jnp.broadcast_to(norm_a, (8, wa))
-    sn_out[:, wa : wa + cb] = jnp.broadcast_to(norm_b, (8, cb))
-    sn_out[:, wa + cb :] = jnp.broadcast_to(end_max, (8, rows))
+    sn_out[0:1, :] = norm_a
+    sn_out[1:2, :] = norm_b[:, 0:wa]
+    sn_out[2:3, :] = norm_b[:, wa:]
+    sn_out[3:8, :] = jnp.broadcast_to(end_max[0:5], (5, rows))
     mirror = ((i + size) % spread, j)
     send(sn_out, sn_in.at[x], st_send.at[1], sn_recv.at[x], mirror)
     send(st_out, st_in.at[x], st_send.at[0], st_recv.at[x], mirror)
@@ -368,7 +370,7 @@
     def _():
         send_weights(straight[0])
 
-    share_weights(in_turn[0])
+    share_weights(in_turn[1])
     arrived(sn_in.at[x], sn_recv.at[x])
     arrived(st_in.at[x], st_recv.at[x])
     send(sn_in.at[x], sn_in.at[x], st_send.at[3], sn_recv.at[x], x_peer)
@@ -380,7 +382,6 @@
         for p in (crossed[2], crossed[3], crossed[1]):
             send_weights(p, first)
 
-    share_weights(in_turn[1])
     arrived(sn_in.at[ox], sn_recv.at[ox])
     arrived(st_in.at[ox], st_recv.at[ox])
 
@@ -401,7 +402,7 @@
         pieces[k] = jnp.where(k == local, own_column, jnp.where(seen, reach, FAR))
         backward_sum = backward_sum + jnp.where(k > local, info[k, 1], 0.0)
     column = jnp.concatenate(pieces, axis=1)
-    past = sn_in[x, :, wa + cb :] + jnp.where(half == 1, forward_sum[0:8], backward_sum[8:16])
+    past = sn_in[x, 3:8, :] + jnp.where(half == 1, forward_sum[0:5], backward_sum[8:13])
     t_at = lax.broadcasted_iota(jnp.int32, (rows, size * rows), 0) + local * rows
     s_at = lax.broadcasted_iota(jnp.int32, (rows, size * rows), 1)
     masks = (s_at <= t_at, s_at >= t_at)
@@ -420,10 +421,10 @@
         queries = query[:, lanes]
         scores = lax.dot_general(queries, keys, nt, preferred_element_type=f32) * width ** (-0.5)
         if row < narrow_heads:
-            memory, normer = st_in[row, 0:wa, :], sn_in[row, 0:1, 0:wa]
+            memory, normer = st_in[row, 0:wa, :], sn_in[row, 0:1, :]
         else:
             memory = jnp.concatenate([st_in[0, wa:, :], st_in[1, wa:, :]], axis=1)
-            normer = sn_in[0, 0:1, wa : wa + cb]
+            normer = jnp.concatenate([sn_in[0, 1:2, :], sn_in[0, 2:3, :]], axis=1)
         recalled = jnp.dot(queries, memory, preferred_element_type=f32) * width ** (-0.5)
         recall_den = jnp.sum(queries.astype(f32) * normer, axis=1, keepdims=True) * width ** (-0.5)
         summed = jnp.zeros((rows, width), f32)
@@ -481,7 +482,7 @@
 
         pass_x(zz, x_send.at[1, zz], x_peer)
 
-    for p in (crossed[2], crossed[3], crossed[1]):
+    for p in (crossed[1], crossed[3], crossed[2]):
         send_weights(p, last)
     share_weights(in_turn[3])
     share_across(i)
@@ -493,8 +494,8 @@
     share_weights(in_turn[6], first)
     share_across(in_turn[3])
     forward_x(2)
+    forward_x(0)
     forward_x(1)
-    forward_x(0)
     for p in in_turn[4:]:
         share_weights(p, last)
     for p in in_turn[4:]:
@@ -600,9 +601,9 @@
         v((depth, own, wide), bf16),
         v((depth, own, wide), bf16),
         v((state_rows, 128), bf16),
-        v((8, state_rows + rows), f32),
+        v((8, rows), f32),
         v((2, state_rows, 128), bf16),
-        v((2, 8, state_rows + rows), f32),
+        v((2, 8, rows), f32),
         dma((spread // 2,)),
         dma((spread // 2,)),
         dma((spread // 2,)),

time: 94.3 us -> 92.9 us (0.985)
  Pallas kernels: 93.5 us -> 92.1 us
    pallas_call x1, Pallas kernels: 93.5 us -> 92.1 us  [fused_shards(): pl.pallas_call(functools.partial(fused_kernel, geometry), out_shape=jax.S...]
where the time goes in v7:
time: 92.9 us; the launch traced here: 92.8 us
  Pallas kernels  92.1 us (99%)
    pallas_call x1, Pallas kernels, fused_shards(): pl.pallas_call(functools.partial(fused_kernel, geometry), out_shape=jax.S...  92.1 us

profile of v7, /device:TPU:0, one launch (start us, length us, event | category | flops | bytes accessed | tf_op | source)
XLA Modules:
  0.0 92.8 jit_solution(5529477161360028345)
XLA Ops:
  0.0 92.1 %fused.1 = bf16[32,2048]{1,0:T(8,128)(2,1)S(1)} custom-call(bf16[128,2048]{1,0:T(8,128)(2,1)} %refs_0_.1, bf16[128,256]{1,0:T(8,128)(2,1)} %refs_1_.1, bf16[128,256]{1,0:T(8,128)(2,1)} %refs_2_.1, bf16[128,256]{1,0:T(8,128)(2,1)} %refs_3_.1, bf16[128,256]{1,0:T(8,128)(2,1)} %refs_4_.1, f32[4,2,128]{2,1,0:T(2,128)} %refs_5_.1, bf16[128,256]{1,0:T(8,128)(2,1)} %refs_6_.1, ...), custom_call_target="tpu_custom_call" | custom-call | tf_op jit(solution)/shard_map/fused/pallas_call | solution.py:632
  92.1 0.7 copy.19

commit v8 on v7

--- a/solution.py
+++ b/solution.py
@@ -521,7 +521,8 @@
         got = jnp.dot(hidden, w_all[2].reshape(units, -1), preferred_element_type=f32)
         part[xx] = got.astype(bf16).reshape(depth, own, -1)
 
-    ends = [(z + depth // 2) % depth] + [(z + k) % depth for k in range(1, depth) if 2 * k != depth]
+    table = ((2, 1, 3), (3, 0, 2), (0, 1, 3), (0, 1, 2))
+    ends = [sum(jnp.where(z == a, table[a][n], 0) for a in range(depth)) for n in range(depth - 1)]
     hidden = hidden_of(ox)
     for p in in_turn[4:]:
         arrived(w_slot(other, p, last), f_recv.at[2, p])

time: 92.9 us -> 92 us (level)
  no operation moved by 1% of the time
where the time goes in v8:
time: 92 us; the launch traced here: 91.9 us
  Pallas kernels  91.2 us (99%)
    pallas_call x1, Pallas kernels, fused_shards(): pl.pallas_call(functools.partial(fused_kernel, geometry), out_shape=jax.S...  91.2 us

profile of v8, /device:TPU:0, one launch (start us, length us, event | category | flops | bytes accessed | tf_op | source)
XLA Modules:
  0.0 91.9 jit_solution(1293778158357076469)
XLA Ops:
  0.0 91.2 %fused.1 = bf16[32,2048]{1,0:T(8,128)(2,1)S(1)} custom-call(bf16[128,2048]{1,0:T(8,128)(2,1)} %refs_0_.1, bf16[128,256]{1,0:T(8,128)(2,1)} %refs_1_.1, bf16[128,256]{1,0:T(8,128)(2,1)} %refs_2_.1, bf16[128,256]{1,0:T(8,128)(2,1)} %refs_3_.1, bf16[128,256]{1,0:T(8,128)(2,1)} %refs_4_.1, f32[4,2,128]{2,1,0:T(2,128)} %refs_5_.1, bf16[128,256]{1,0:T(8,128)(2,1)} %refs_6_.1, ...), custom_call_target="tpu_custom_call" | custom-call | tf_op jit(solution)/shard_map/fused/pallas_call | solution.py:633
  91.2 0.7 copy.19

commit v9 on v8

--- a/solution.py
+++ b/solution.py
@@ -382,6 +382,7 @@
         for p in (crossed[2], crossed[3], crossed[1]):
             send_weights(p, first)
 
+    share_weights(in_turn[2])
     arrived(sn_in.at[ox], sn_recv.at[ox])
     arrived(st_in.at[ox], st_recv.at[ox])
 
@@ -451,7 +452,6 @@
     for k in range(1, members):
         q = (j + k) % members
         send(pp.at[q], rs.at[j], p_send.at[q], p_recv.at[j], (i, q))
-    share_weights(in_turn[2])
     stream = res[pl.ds(pl.multiple_of(j * own, own), own), :].astype(f32) + pp[j].astype(f32)
     for k in range(1, members):
         q = (j + k) % members
@@ -521,7 +521,7 @@
         got = jnp.dot(hidden, w_all[2].reshape(units, -1), preferred_element_type=f32)
         part[xx] = got.astype(bf16).reshape(depth, own, -1)
 
-    table = ((2, 1, 3), (3, 0, 2), (0, 1, 3), (0, 1, 2))
+    table = ((2, 3, 1), (3, 0, 2), (0, 1, 3), (0, 1, 2))
     ends = [sum(jnp.where(z == a, table[a][n], 0) for a in range(depth)) for n in range(depth - 1)]
     hidden = hidden_of(ox)
     for p in in_turn[4:]:

time: 92 us -> 92.2 us (level)
  no operation moved by 1% of the time
where the time goes in v9:
time: 92.2 us; the launch traced here: 92 us
  Pallas kernels  91.4 us (99%)
    pallas_call x1, Pallas kernels, fused_shards(): pl.pallas_call(functools.partial(fused_kernel, geometry), out_shape=jax.S...  91.4 us

profile of v9, /device:TPU:0, one launch (start us, length us, event | category | flops | bytes accessed | tf_op | source)
XLA Modules:
  0.0 92.0 jit_solution(13725226652926442796)
XLA Ops:
  0.0 91.4 %fused.1 = bf16[32,2048]{1,0:T(8,128)(2,1)S(1)} custom-call(bf16[128,2048]{1,0:T(8,128)(2,1)} %refs_0_.1, bf16[128,256]{1,0:T(8,128)(2,1)} %refs_1_.1, bf16[128,256]{1,0:T(8,128)(2,1)} %refs_2_.1, bf16[128,256]{1,0:T(8,128)(2,1)} %refs_3_.1, bf16[128,256]{1,0:T(8,128)(2,1)} %refs_4_.1, f32[4,2,128]{2,1,0:T(2,128)} %refs_5_.1, bf16[128,256]{1,0:T(8,128)(2,1)} %refs_6_.1, ...), custom_call_target="tpu_custom_call" | custom-call | tf_op jit(solution)/shard_map/fused/pallas_call | solution.py:633
  91.4 0.7 copy.19
